TPU v7x, 256 devices: a whole 4x4x8 slice. The times are simulated.
256 devices in a mesh: sp: 16 (over y, x), tp: 16 (over z, core).
Axes of the slice: x: 4, y: 4, z: 8, core: 2. Of those that a mesh axis runs over, the one named last changes fastest.
Arguments:
- queries: bfloat16 [32768, 2048], P('sp', 'tp'), may hold values from -160 to 160
- key_heads: bfloat16 [32768, 512], P('sp'), may hold values from -8 to 8
- value_heads: bfloat16 [32768, 512], P('sp'), may hold values from -4 to 4
- sink_logit: float32 [16], P('tp'), may hold values from -2 to 7
- out_weight: bfloat16 [2048, 2048], P('tp'), may hold values from -0.125 to 0.125
- residual: bfloat16 [32768, 2048], P(('sp', 'tp')), may hold values from -6 to 6
- mixer_gain: float32 [2048], replicated, may hold values from 0.1 to 1.9
- expert_gain: float32 [2048], replicated, may hold values from 0.1 to 1.9
- route_group: int32 [32768], P(('sp', 'tp')), may hold values from 0 to 15, as said below
- route_member: int32 [32768, 2], P(('sp', 'tp')), may hold values from 0 to 2, as said below
- route_weight: bfloat16 [32768, 2], P(('sp', 'tp')), may hold values from 0.19921875 to 1
- gate_weight: bfloat16 [48, 2048, 2048], P('sp', None, 'tp'), may hold values from -0.125 to 0.125
- up_weight: bfloat16 [48, 2048, 2048], P('sp', None, 'tp'), may hold values from -0.125 to 0.125
- down_weight: bfloat16 [48, 2048, 2048], P('sp', 'tp'), may hold values from -0.125 to 0.125
Outputs:
- output: bfloat16 [32768, 2048], P(('sp', 'tp'))
Inputs may be any that keep to these rules, and one draw needn't show every extreme that they name: `route_group`: among the tokens of one device, at most 10 name one group; in every draw one group is named by exactly 10 tokens of every device. `route_member`: the two entries of a token are different members of its group.
All inputs are finite; a program needn't handle non-finite values.
Results may differ from a plain program's by a relative error of at most 0.018.
Values may be sent and summed in bfloat16 or wider, within the bound.
No kernel may reach another device: no remote copies, remote signals or barrier semaphores. Data moves between devices by JAX's collectives and lax.ppermute only.
A program may use at most 128 MiB of HBM per device.

v0:
```python
import jax
import jax.numpy as jnp
from jax import lax
from jax.sharding import Mesh
from jax.sharding import PartitionSpec as P

HEADS = 16
KV_HEADS = 4
HEAD_DIM = 128
WINDOW = 128
BLOCK = 128
GROUP_EXPERTS = 3
TP = ("tp_0", "tp_1")
SP_TP = ("sp", "tp_0", "tp_1")


EPS = 1e-06
NEG_BIG = -1e30


def extended(block, sides, width):
    for axis, dim in sides:
        count = lax.axis_size(axis)
        forward = [(i, i + 1) for i in range(count - 1)]
        backward = [(target, source) for source, target in forward]
        low = lax.ppermute(
            lax.slice_in_dim(block, block.shape[dim] - width, None, axis=dim), axis, forward
        )
        high = lax.ppermute(lax.slice_in_dim(block, 0, width, axis=dim), axis, backward)
        block = jnp.concatenate([low, block, high], axis=dim)
    return block


def cut_along(shard, dim, devices):
    dims = shard.shape
    blocks = shard.reshape(*dims[:dim], devices, dims[dim] // devices, *dims[dim + 1 :])
    return jnp.moveaxis(blocks, dim, 0)


def joined_along(blocks, dim):
    dims = list(blocks.shape[1:])
    dims[dim] *= blocks.shape[0]
    return jnp.moveaxis(blocks, 0, dim).reshape(dims)


def exchange_in_order(blocks, axes, order):
    dims = [lax.axis_size(a) for a in axes]
    blocks = blocks.reshape(*dims, *blocks.shape[1:])
    for k in order:
        blocks = lax.all_to_all(blocks, axes[k], split_axis=k, concat_axis=k, tiled=True)
    return blocks.reshape(-1, *blocks.shape[len(axes) :])


def stepwise_exchange(shard, axes, order, split_dim, concat_dim):
    blocks = cut_along(shard, split_dim, lax.axis_size(axes))
    return joined_along(exchange_in_order(blocks, axes, order), concat_dim)


def window_attention(queries, key_heads, value_heads, sink_logit):
    seq_rows = queries.shape[0]
    heads_dev = sink_logit.shape[0]
    key_group = HEADS // KV_HEADS
    key_start = lax.axis_index(TP) * heads_dev // key_group * HEAD_DIM
    key_own = lax.dynamic_slice_in_dim(key_heads, key_start, HEAD_DIM, 1)
    value_own = lax.dynamic_slice_in_dim(value_heads, key_start, HEAD_DIM, 1)
    padded = extended(jnp.stack([key_own, value_own]), (("sp", 1),), WINDOW)
    blocks = seq_rows // BLOCK
    extent = WINDOW // BLOCK
    tile_rows = padded.reshape(2, blocks + 2 * extent, BLOCK, HEAD_DIM)
    key_spans = jnp.concatenate(
        [tile_rows[:, shifted : shifted + blocks] for shifted in range(2 * extent + 1)], axis=2
    )
    offset = lax.axis_index("sp") * seq_rows
    seq_total = seq_rows * lax.axis_size("sp")
    query_pos = offset + jnp.arange(seq_rows, dtype=jnp.int32).reshape(blocks, BLOCK)
    key_pos = (
        offset
        + (jnp.arange(blocks, dtype=jnp.int32) * BLOCK)[:, None]
        + jnp.arange(BLOCK + 2 * WINDOW, dtype=jnp.int32)[None, :]
        - WINDOW
    )
    inside = (
        (jnp.abs(query_pos[:, :, None] - key_pos[:, None, :]) <= WINDOW)
        & (key_pos >= 0)[:, None, :]
        & (key_pos < seq_total)[:, None, :]
    )
    query_blocks = queries.reshape(blocks, BLOCK, heads_dev, HEAD_DIM)
    scores = jnp.einsum(
        "nqhd,nkd->nhqk", query_blocks, key_spans[0], preferred_element_type=jnp.float32
    ) * HEAD_DIM ** (-0.5)
    scores = jnp.where(inside[:, None], scores, NEG_BIG)
    sink_col = sink_logit[None, :, None, None]
    row_top = jnp.maximum(jnp.max(scores, axis=3, keepdims=True), sink_col)
    exp_terms = jnp.exp(scores - row_top)
    row_mass = jnp.sum(exp_terms, axis=3, keepdims=True) + jnp.exp(sink_col - row_top)
    weight = (exp_terms / row_mass).astype(jnp.bfloat16)
    attended = jnp.einsum(
        "nhqk,nkd->nqhd", weight, key_spans[1], preferred_element_type=jnp.float32
    ).astype(jnp.bfloat16)
    return attended.reshape(seq_rows, heads_dev * HEAD_DIM)


def per_device(
    queries,
    key_heads,
    value_heads,
    sink_logit,
    out_weight,
    residual,
    mixer_gain,
    expert_gain,
    route_group,
    route_member,
    route_weight,
    gate_weight,
    up_weight,
    down_weight,
):
    attended = window_attention(queries, key_heads, value_heads, sink_logit)
    tok_rows = residual.shape[0]
    width = out_weight.shape[1]
    by_token = stepwise_exchange(attended, TP, (1, 0), 0, 1)
    shard_rows = out_weight.shape[0]
    weight_piece = lax.all_gather(out_weight, TP, axis=0, tiled=True)
    shards = weight_piece.shape[0] // shard_rows
    columns = by_token
    columns = columns.reshape(tok_rows, shards, shard_rows)
    weight_slabs = weight_piece.reshape(shards, shard_rows, width)
    products = jnp.einsum("rkc,kcd->krd", columns, weight_slabs, preferred_element_type=jnp.float32)
    rounded = lax.optimization_barrier(products.astype(jnp.bfloat16))
    projected = jnp.sum(rounded.astype(jnp.float32), axis=0)
    proj_scale = lax.rsqrt(jnp.mean(projected * projected, axis=1, keepdims=True) + EPS)
    mixed_rows = (residual.astype(jnp.float32) + mixer_gain * (projected * proj_scale)).astype(
        jnp.bfloat16
    )
    mixed_float = mixed_rows.astype(jnp.float32)
    norm_scale = lax.rsqrt(jnp.mean(mixed_float * mixed_float, axis=1, keepdims=True) + EPS)
    normed = (mixed_float * norm_scale * expert_gain).astype(jnp.bfloat16)
    groups = lax.axis_size("sp")
    capacity = max(2, (5 * tok_rows + 4 * groups - 1) // (4 * groups))
    group_ids = jnp.arange(groups, dtype=jnp.int32)
    chosen = (route_group[:, None] == group_ids[None, :]).astype(jnp.int32)
    group_rank = jnp.sum(chosen * (jnp.cumsum(chosen, axis=0) - 1), axis=1)
    slot_ids = route_group * capacity + group_rank
    placing = (jnp.arange(groups * capacity, dtype=jnp.int32)[:, None] == slot_ids[None, :]).astype(
        jnp.bfloat16
    )
    member_ids = jnp.arange(GROUP_EXPERTS, dtype=jnp.int32)
    token_gates = jnp.sum(
        route_weight.astype(jnp.float32)[:, :, None]
        * (route_member[:, :, None] == member_ids[None, None, :]).astype(jnp.float32),
        axis=1,
    ).astype(jnp.bfloat16)
    send_rows = (
        jnp.dot(placing, normed, preferred_element_type=jnp.float32)
        .astype(jnp.bfloat16)
        .reshape(groups, capacity, width)
    )
    send_gates = (
        jnp.dot(placing, token_gates, preferred_element_type=jnp.float32)
        .astype(jnp.bfloat16)
        .reshape(groups, capacity, GROUP_EXPERTS)
    )
    arrived_rows, arrived_gates = (
        lax.all_to_all(send_rows, "sp", split_axis=0, concat_axis=0, tiled=True),
        lax.all_to_all(send_gates, "sp", split_axis=0, concat_axis=0, tiled=True),
    )
    pooled_rows, pooled_gates = (
        lax.all_gather(arrived_rows, TP, axis=0, tiled=True),
        lax.all_gather(arrived_gates, TP, axis=0, tiled=True),
    )
    flat_rows = pooled_rows.reshape(-1, width)
    flat_gates = pooled_gates.reshape(-1, GROUP_EXPERTS).astype(jnp.float32)
    gate_pre = jnp.einsum("md,edh->meh", flat_rows, gate_weight, preferred_element_type=jnp.float32)
    up_pre = jnp.einsum("md,edh->meh", flat_rows, up_weight, preferred_element_type=jnp.float32)
    hidden = (jax.nn.silu(gate_pre) * up_pre * flat_gates[:, :, None]).astype(jnp.bfloat16)
    partial_out = jnp.einsum("meh,ehd->md", hidden, down_weight, preferred_element_type=jnp.float32)
    summed = lax.psum_scatter(
        partial_out.reshape(pooled_rows.shape).astype(jnp.bfloat16),
        TP,
        scatter_dimension=0,
        tiled=True,
    )
    returned = lax.all_to_all(summed, "sp", split_axis=0, concat_axis=0, tiled=True)
    expert_out = lax.dot_general(
        placing,
        returned.reshape(groups * capacity, width),
        (((0,), (0,)), ((), ())),
        preferred_element_type=jnp.float32,
    )
    return (mixed_float + expert_out).astype(jnp.bfloat16)


def solution(mesh):
    torus = Mesh(mesh.devices.reshape(mesh.shape["sp"], 8, 2), ("sp", "tp_0", "tp_1"))
    placed = (
        P("sp", TP),
        P("sp", None),
        P("sp", None),
        P(TP),
        P(TP, None),
        P(SP_TP, None),
        P(),
        P(),
        P(SP_TP),
        P(SP_TP, None),
        P(SP_TP, None),
        P("sp", None, TP),
        P("sp", None, TP),
        P("sp", TP, None),
    )
    return jax.shard_map(
        per_device, mesh=torus, in_specs=placed, out_specs=P(SP_TP, None), check_vma=False
    )
```

profile of v0, /device:TPU:1, one launch (start us, length us, event | category | flops | bytes accessed | tf_op | source)
XLA Modules:
  0.0 386.0 jit_solution(15848808001674454527)
XLA Ops:
  6.5 0.0 copy-start
  6.5 0.0 all-gather.3.cloned.1.call-start
  6.5 0.7 all-gather.3.cloned.1.call-update
  7.3 1.3 dynamic-slice_bitcast_fusion
  8.6 3.9 %collective-permute-start = (bf16[2,128,128]{2,1,0:T(8,128)(2,1)S(1)}, bf16[2,128,128]{2,1,0:T(8,128)(2,1)S(1)}, u32[]{:S(2)}, u32[]{:S(2)}) collective-permute-start(bf16[2,128,128]{2,1,0:T(8,128)(2,1)S(1)} %get-tuple-element.10), channel_id=1, source_target_pairs={{0,16},{16,32},{32,48},{48,64},{64,80},{80,96},{96,112},{112,128},... | collective-permute-start | bytes 196616 | tf_op jit(solution)/shard_map/ppermute | solution.py:26
  12.5 1.3 collective-permute-start.1
  14.5 0.1 fusion.22
  14.6 0.1 add_add_fusion
  14.7 0.0 collective-permute-done
  14.7 2.9 collective-permute-done.1
  17.5 0.1 pad_maximum_fusion.1
  17.6 0.8 fusion.25
  18.4 0.0 copy-start.6
  18.4 0.4 pad_maximum_fusion
  18.8 0.6 copy-done.6
  19.5 4.1 %fusion.26 = (f32[16,128]{1,0:T(8,128)S(1)}, f32[16,1,128,384]{2,3,0,1:T(8,128)S(1)}) fusion(bf16[16,128,128]{2,1,0:T(8,128)(2,1)S(1)} %bitcast.66, bf16[2,16,384,128]{3,2,1,0:T(8,128)(2,1)S(1)} %pad_maximum_fusion, pred[16,384]{1,0:T(8,128)(4,1)S(1)} %get-tuple-element.13, pred[16,384]{1,0:T(8,128)(4,1)S(1)} %get-tuple-element.12, ...), kind=kOutput, calls=%fused_computation.58 | convolution fusion | flops 207616000 | bytes 5296128 | tf_op jit(solution)/shard_map/nqhd,nkd->nhqk/dot_general | solution.py:88
  23.6 0.4 fusion.4
  24.0 1.0 fusion.8
  25.1 0.0 copy-start.4
  25.2 5.9 %all_to_all.25 = bf16[8,2,128,128]{2,3,0,1:T(8,128)(2,1)S(1)} all-to-all(bf16[8,2,128,128]{2,3,0,1:T(8,128)(2,1)S(1)} %copy.57), channel_id=1, replica_groups=mesh['sp'=16,'tp_0'=8,'tp_1'=2] {'tp_1'}, dimensions={1} | all-to-all | bytes 1048576 | tf_op jit(solution)/shard_map/all_to_all | solution.py:50
  31.0 0.8 copy.58
  31.9 8.2 %all-to-all-start.1 = ((bf16[8,2,128,128]{2,3,1,0:T(8,128)(2,1)}), bf16[8,2,128,128]{2,3,1,0:T(8,128)(2,1)S(1)}, u32[]{:S(2)}, u32[]{:S(2)}) async-start(bf16[8,2,128,128]{2,3,1,0:T(8,128)(2,1)} %copy.58), calls=%async_computation.1 | async-start | bytes 1048576 | tf_op jit(solution)/shard_map/all_to_all | solution.py:50
  40.1 0.0 all-gather.5.cloned.1.call-start
  40.1 0.0 copy-done.4
  40.1 0.1 fusion.17
  40.2 0.2 reduce_window_sum.11
  40.4 0.2 select_reduce_fusion
  40.6 22.8 %all-to-all-done.1 = bf16[8,2,128,128]{2,3,1,0:T(8,128)(2,1)S(1)} async-done(((bf16[8,2,128,128]{2,3,1,0:T(8,128)(2,1)}), bf16[8,2,128,128]{2,3,1,0:T(8,128)(2,1)S(1)}, u32[]{:S(2)}, u32[]{:S(2)}) %all-to-all-start.1) | async-done | bytes 524320 | tf_op jit(solution)/shard_map/all_to_all | solution.py:50
  63.4 0.3 copy.59
  63.7 16.8 %all-gather.3.cloned.1.call-done = bf16[2048,2048]{1,0:T(8,128)(2,1)} async-done(((bf16[128,2048]{1,0:T(8,128)(2,1)}), bf16[2048,2048]{1,0:T(8,128)(2,1)}) %all-gather.3.cloned.1.call-update) | async-done | bytes 8388624 | tf_op jit(solution)/shard_map/all_gather | solution.py:124
  80.5 5.7 %convolution_convert_fusion = bf16[16,128,2048]{2,1,0:T(8,128)(2,1)S(1)} fusion(bf16[128,16,128]{2,0,1:T(8,128)(2,1)S(1)} %bitcast.64, bf16[16,128,2048]{2,1,0:T(8,128)(2,1)} %bitcast.62), kind=kOutput, calls=%fused_computation.2 | convolution fusion | flops 1077936128 | bytes 17301504 | tf_op jit(solution)/shard_map/rkc,kcd->krd/dot_general | solution.py:129
  86.2 0.0 copy-start.1
  86.2 0.0 copy-start.2
  86.3 1.8 convert_reduce_fusion
  88.1 0.0 copy-start.3
  88.1 0.2 multiply_reduce_fusion
  88.3 0.0 copy-done.1
  88.3 0.0 copy-done.2
  88.3 0.4 fusion.11
  88.7 0.1 copy-done.3
  88.8 1.3 convolution_convert_fusion.1
  90.1 1.3 reshape.189
  91.4 22.8 %all_to_all.26 = bf16[16,10,2048]{2,1,0:T(8,128)(2,1)S(1)} all-to-all(bf16[16,10,2048]{2,1,0:T(8,128)(2,1)S(1)} %reshape.189), channel_id=1, replica_groups=mesh['sp'=16,'tp_0'=8,'tp_1'=2] {'sp'}, dimensions={0} | all-to-all | bytes 1310720 | tf_op jit(solution)/shard_map/all_to_all | solution.py:165
  114.2 1.2 copy.60
  115.4 0.0 all-gather.5.cloned.1.call-update
  115.4 0.0 reduce-scatter.2.cloned.1.call-start
  115.5 0.1 convolution_convert_fusion.2
  115.7 0.1 reshape.191
  115.8 9.6 %all_to_all.27 = bf16[16,10,3]{1,2,0:T(4,128)(2,1)S(1)} all-to-all(bf16[16,10,3]{1,2,0:T(4,128)(2,1)S(1)} %copy.62), channel_id=1, replica_groups=mesh['sp'=16,'tp_0'=8,'tp_1'=2] {'sp'}, dimensions={0} | all-to-all | bytes 1920 | tf_op jit(solution)/shard_map/all_to_all | solution.py:166
  125.4 20.6 %all_gather.11 = bf16[256,10,3]{1,2,0:T(4,128)(2,1)S(1)} all-gather(bf16[16,10,3]{1,2,0:T(4,128)(2,1)S(1)} %all_to_all.27), channel_id=1, replica_groups=mesh['sp'=16,'tp_0'=8,'tp_1'=2] {'tp_0','tp_1'}, dimensions={0}, use_global_device_ids=true | all-gather | bytes 16320 | tf_op jit(solution)/shard_map/all_gather | solution.py:170
  146.0 0.2 copy.63
  146.2 0.2 copy.64
  146.3 0.3 reshape.193
  146.6 32.3 %all-gather.5.cloned.1.call-done = bf16[256,10,2048]{2,0,1:T(8,128)(2,1)} async-done(((bf16[16,10,2048]{2,0,1:T(8,128)(2,1)}), bf16[256,10,2048]{2,0,1:T(8,128)(2,1)}) %all-gather.5.cloned.1.call-update) | async-done | bytes 10485776 | tf_op jit(solution)/shard_map/all_gather | solution.py:169
  178.9 15.4 %copy.61 = bf16[256,10,2048]{2,1,0:T(8,128)(2,1)} copy(bf16[256,10,2048]{2,0,1:T(8,128)(2,1)} %all-gather.5.cloned.1.call-done) | data formatting | bytes 20971520 | tf_op jit(solution)/shard_map/all_gather | solution.py:169
  194.3 18.1 %reshape.194 = bf16[2560,2048,1]{1,0,2:T(8,128)(2,1)} reshape(bf16[256,10,2048]{2,1,0:T(8,128)(2,1)} %copy.61) | data formatting | bytes 20971520 | tf_op jit(solution)/shard_map/reshape | solution.py:172
  212.4 10.0 %fusion.27 = f32[2560,3,128]{2,0,1:T(8,128)} fusion(bf16[2560,2048,1]{1,0,2:T(8,128)(2,1)} %reshape.194, bf16[3,2048,128]{2,1,0:T(8,128)(2,1)} %param.25), kind=kOutput, calls=%fused_computation.59 | convolution fusion | flops 4026531840 | bytes 15990784 | tf_op jit(solution)/shard_map/md,edh->meh/dot_general | solution.py:174
  222.4 16.4 %bitcast_convert_fusion = bf16[2560,2048]{1,0:T(8,128)(2,1)} fusion(bf16[3,128,2048]{2,1,0:T(8,128)(2,1)S(1)} %copy-done, bf16[2560,2048,1]{1,0,2:T(8,128)(2,1)} %reshape.194, bf16[3,2048,128]{2,1,0:T(8,128)(2,1)} %param.26, f32[2560,3,128]{2,0,1:T(8,128)} %fusion.27, f32[2560,3]{0,1:T(4,128)S(1)} %reshape.193), kind=kOutput, calls=%fused_computation | convolution fusion | flops 8065187840 | bytes 28080128 | tf_op jit(solution)/shard_map/meh,ehd->md/dot_general | solution.py:177
  238.8 17.7 %convert_element_type.88 = bf16[256,10,2048]{2,1,0:T(8,128)(2,1)} reshape(bf16[2560,2048]{1,0:T(8,128)(2,1)} %bitcast_convert_fusion) | data formatting | bytes 20971520 | tf_op jit(solution)/shard_map/convert_element_type | solution.py:179
  256.5 0.0 reduce-scatter.2.cloned.1.call-update
  256.5 97.8 %reduce-scatter.2.cloned.1.call-done = bf16[16,10,2048]{2,1,0:T(8,128)(2,1)} async-done(((bf16[256,10,2048]{2,1,0:T(8,128)(2,1)}), bf16[16,10,2048]{2,1,0:T(8,128)(2,1)}) %reduce-scatter.2.cloned.1.call-update) | async-done | bytes 655376 | tf_op jit(solution)/shard_map/reduce_scatter | solution.py:178
  354.3 21.9 %all_to_all.28 = bf16[16,10,2048]{2,1,0:T(8,128)(2,1)S(1)} all-to-all(bf16[16,10,2048]{2,1,0:T(8,128)(2,1)} %reduce-scatter.2.cloned.1.call-done), channel_id=1, replica_groups=mesh['sp'=16,'tp_0'=8,'tp_1'=2] {'sp'}, dimensions={0} | all-to-all | bytes 1310720 | tf_op jit(solution)/shard_map/all_to_all | solution.py:184
  376.1 1.1 reshape.192
  377.2 2.2 fusion.5
  (17 shorter events, 0.1 us)
Async XLA Ops:
  6.5 215.9 %copy-start = (bf16[3,128,2048]{2,1,0:T(8,128)(2,1)S(1)}, bf16[3,128,2048]{2,1,0:T(8,128)(2,1)}, u32[]{:S(2)}) copy-start(bf16[3,128,2048]{2,1,0:T(8,128)(2,1)} %param.27) | copy-start | bytes 4718596
  6.5 74.0 %all-gather.3.cloned.1.call-start = ((), (), s32[]{:S(2)}) async-start(), calls=%async_computation.6 | async-start | bytes 8912896 | tf_op jit(solution)/shard_map/all_gather | solution.py:124
  8.6 6.1 %collective-permute-start = (bf16[2,128,128]{2,1,0:T(8,128)(2,1)S(1)}, bf16[2,128,128]{2,1,0:T(8,128)(2,1)S(1)}, u32[]{:S(2)}, u32[]{:S(2)}) collective-permute-start(bf16[2,128,128]{2,1,0:T(8,128)(2,1)S(1)} %get-tuple-element.10), channel_id=1, source_target_pairs={{0,16},{16,32},{32,48},{48,64},{64,80},{80,96},{96,112},{112,128},... | collective-permute-start | bytes 196616 | tf_op jit(solution)/shard_map/ppermute | solution.py:26
  12.5 5.0 %collective-permute-start.1 = (bf16[2,128,128]{2,1,0:T(8,128)(2,1)S(1)}, bf16[2,128,128]{2,1,0:T(8,128)(2,1)S(1)}, u32[]{:S(2)}, u32[]{:S(2)}) collective-permute-start(bf16[2,128,128]{2,1,0:T(8,128)(2,1)S(1)} %get-tuple-element.11), channel_id=1, source_target_pairs={{16,0},{32,16},{48,32},{64,48},{80,64},{96,80},{112,96},{128,112},... | collective-permute-start | bytes 196616 | tf_op jit(solution)/shard_map/ppermute | solution.py:29
  18.4 1.0 copy-start.6
  25.1 15.0 %copy-start.4 = (s32[128]{0:T(128)S(1)}, s32[128]{0:T(128)}, u32[]{:S(2)}) copy-start(s32[128]{0:T(128)} %param.22) | copy-start | bytes 1540
  31.9 31.5 %all-to-all-start.1 = ((bf16[8,2,128,128]{2,3,1,0:T(8,128)(2,1)}), bf16[8,2,128,128]{2,3,1,0:T(8,128)(2,1)S(1)}, u32[]{:S(2)}, u32[]{:S(2)}) async-start(bf16[8,2,128,128]{2,3,1,0:T(8,128)(2,1)} %copy.58), calls=%async_computation.1 | async-start | bytes 1048576 | tf_op jit(solution)/shard_map/all_to_all | solution.py:50
  40.1 138.9 %all-gather.5.cloned.1.call-start = ((), (), s32[]{:S(2)}) async-start(), calls=%async_computation.7 | async-start | bytes 11141120 | tf_op jit(solution)/shard_map/all_gather | solution.py:169
  86.2 2.1 copy-start.1
  86.2 2.0 copy-start.2
  88.1 0.7 copy-start.3
  90.1 25.4 %copy-start.7 = (bf16[128,2]{0,1:T(2,128)(2,1)S(1)}, bf16[128,2]{0,1:T(2,128)(2,1)}, u32[]{:S(2)}) copy-start(bf16[128,2]{0,1:T(2,128)(2,1)} %param.24) | copy-start | bytes 1540
  90.1 25.4 %copy-start.5 = (s32[128,2]{0,1:T(2,128)S(1)}, s32[128,2]{0,1:T(2,128)}, u32[]{:S(2)}) copy-start(s32[128,2]{0,1:T(2,128)} %param.23) | copy-start | bytes 3076
  115.4 238.8 %reduce-scatter.2.cloned.1.call-start = ((), (), s32[]{:S(2)}) async-start(), calls=%async_computation.8 | async-start | bytes 17825792 | tf_op jit(solution)/shard_map/reduce_scatter | solution.py:178
Sparse Core Ops, SparseCore 0:
  9.2 71.3 all-gather.2
  115.5 63.3 all-gather.4
  256.6 97.6 reduce-scatter.1
where the time goes:
time: 389 us; the launch traced here: 386 us
  waiting for transfers between devices  173 us (44%)
  blocking collectives  80.7 us (21%)
  local copies, waits for them, and re-layouts  59.5 us (15%)
  matrix products  40.9 us (11%)
  between operations  14.1 us (4%)
  starting transfers between devices  13.5 us (3%)
  other arithmetic  3.92 us (1%)
    reduce_scatter x1, waiting for transfers between devices, per_device(): lax.psum_scatter(partial_out.reshape(pooled_rows.shape).astype(jnp.bfloat...  97.8 us
    all_gather x1, waiting for transfers between devices, per_device(): lax.all_gather(arrived_rows, TP, axis=0, tiled=True)  32.3 us
    all_to_all x1, waiting for transfers between devices, exchange_in_order(): lax.all_to_all(blocks, axes[k], split_axis=k, concat_axis=k, tiled=True)  22.8 us
    all_to_all x1, blocking collectives, per_device(): lax.all_to_all(send_rows, 'sp', split_axis=0, concat_axis=0, tiled=True)  22.8 us
    all_to_all x1, blocking collectives, per_device(): lax.all_to_all(summed, 'sp', split_axis=0, concat_axis=0, tiled=True)  21.9 us
    all_gather x1, blocking collectives, per_device(): lax.all_gather(arrived_gates, TP, axis=0, tiled=True)  20.6 us
    reshape x1, local copies, waits for them, and re-layouts, per_device(): flat_rows = pooled_rows.reshape(-1, width)  18.1 us
    convert_element_type x1, local copies, waits for them, and re-layouts, per_device(): partial_out.reshape(pooled_rows.shape).astype(jnp.bfloat16)  17.7 us
  transfers between devices with their start and end apart: 6, of which 5 were waited for; matrix products, arithmetic and copies ran while one was open for 3% of the time, Pallas kernels for 0%

commit v1 on v0

v1 whole, which is shorter than its diff:
```python
import jax
import jax.numpy as jnp
from jax import lax
from jax.sharding import Mesh
from jax.sharding import PartitionSpec as P

HEADS = 16
KV_HEADS = 4
HEAD_DIM = 128
WINDOW = 128
BLOCK = 128
GROUP_EXPERTS = 3
GROUP_CAP = 10
LANES = 128
Z = "tp_0"
CORE = "tp_1"
TP = (Z, CORE)
SP_TP = ("sp", Z, CORE)
SWAP = [(0, 1), (1, 0)]

EPS = 1e-06
NEG_BIG = -1e30


def extended(block, width):
    count = lax.axis_size("sp")
    forward = [(i, i + 1) for i in range(count - 1)]
    backward = [(target, source) for source, target in forward]
    low = lax.ppermute(block[:, block.shape[1] - width :], "sp", forward)
    high = lax.ppermute(block[:, :width], "sp", backward)
    return jnp.concatenate([low, block, high], axis=1)


def window_attention(queries, key_heads, value_heads, sink_logit):
    seq_rows = queries.shape[0]
    heads_dev = sink_logit.shape[0]
    key_group = HEADS // KV_HEADS
    key_start = lax.axis_index(TP) * heads_dev // key_group * HEAD_DIM
    key_own = lax.dynamic_slice_in_dim(key_heads, key_start, HEAD_DIM, 1)
    value_own = lax.dynamic_slice_in_dim(value_heads, key_start, HEAD_DIM, 1)
    padded = extended(jnp.stack([key_own, value_own]), WINDOW)
    blocks = seq_rows // BLOCK
    extent = WINDOW // BLOCK
    tile_rows = padded.reshape(2, blocks + 2 * extent, BLOCK, HEAD_DIM)
    key_spans = jnp.concatenate(
        [tile_rows[:, shifted : shifted + blocks] for shifted in range(2 * extent + 1)], axis=2
    )
    offset = lax.axis_index("sp") * seq_rows
    seq_total = seq_rows * lax.axis_size("sp")
    query_pos = offset + jnp.arange(seq_rows, dtype=jnp.int32).reshape(blocks, BLOCK)
    key_pos = (
        offset
        + (jnp.arange(blocks, dtype=jnp.int32) * BLOCK)[:, None]
        + jnp.arange(BLOCK + 2 * WINDOW, dtype=jnp.int32)[None, :]
        - WINDOW
    )
    inside = (
        (jnp.abs(query_pos[:, :, None] - key_pos[:, None, :]) <= WINDOW)
        & (key_pos >= 0)[:, None, :]
        & (key_pos < seq_total)[:, None, :]
    )
    query_blocks = queries.reshape(blocks, BLOCK, heads_dev, HEAD_DIM)
    scores = jnp.einsum(
        "nqhd,nkd->nhqk", query_blocks, key_spans[0], preferred_element_type=jnp.float32
    ) * HEAD_DIM ** (-0.5)
    scores = jnp.where(inside[:, None], scores, NEG_BIG)
    sink_col = sink_logit[None, :, None, None]
    row_top = jnp.maximum(jnp.max(scores, axis=3, keepdims=True), sink_col)
    exp_terms = jnp.exp(scores - row_top)
    row_mass = jnp.sum(exp_terms, axis=3, keepdims=True) + jnp.exp(sink_col - row_top)
    weight = (exp_terms / row_mass).astype(jnp.bfloat16)
    attended = jnp.einsum(
        "nhqk,nkd->nqhd", weight, key_spans[1], preferred_element_type=jnp.float32
    ).astype(jnp.bfloat16)
    return attended.reshape(seq_rows, heads_dev * HEAD_DIM)


def per_device(
    queries,
    key_heads,
    value_heads,
    sink_logit,
    out_weight,
    residual,
    mixer_gain,
    expert_gain,
    route_group,
    route_member,
    route_weight,
    gate_weight,
    up_weight,
    down_weight,
):
    depth = lax.axis_size(Z)
    groups = lax.axis_size("sp")
    core = lax.axis_index(CORE)
    tok_rows, width = residual.shape
    capacity = GROUP_CAP
    slots = groups * capacity

    weight_rows = lax.all_gather(out_weight, Z, axis=0, tiled=False)
    attended = window_attention(queries, key_heads, value_heads, sink_logit)
    by_chip = lax.all_to_all(
        attended.reshape(depth, 2, tok_rows, HEAD_DIM), Z, split_axis=0, concat_axis=0, tiled=True
    )

    def head_sum(which):
        rows = lax.dynamic_index_in_dim(by_chip, which, 1, False)
        return jnp.einsum("zrk,zkn->rn", rows, weight_rows, preferred_element_type=jnp.float32)

    from_partner = lax.ppermute(head_sum(1 - core).astype(jnp.bfloat16), CORE, SWAP)
    projected = head_sum(core) + from_partner.astype(jnp.float32)
    proj_scale = lax.rsqrt(jnp.mean(projected * projected, axis=1, keepdims=True) + EPS)
    mixed_rows = (residual.astype(jnp.float32) + mixer_gain * (projected * proj_scale)).astype(
        jnp.bfloat16
    )
    mixed_float = mixed_rows.astype(jnp.float32)
    norm_scale = lax.rsqrt(jnp.mean(mixed_float * mixed_float, axis=1, keepdims=True) + EPS)
    normed = (mixed_float * norm_scale * expert_gain).astype(jnp.bfloat16)

    group_ids = jnp.arange(groups, dtype=jnp.int32)
    chosen = (route_group[:, None] == group_ids[None, :]).astype(jnp.int32)
    group_rank = jnp.sum(chosen * (jnp.cumsum(chosen, axis=0) - 1), axis=1)
    slot_ids = route_group * capacity + group_rank
    placing = (jnp.arange(slots, dtype=jnp.int32)[:, None] == slot_ids[None, :]).astype(
        jnp.bfloat16
    )
    member_ids = jnp.arange(GROUP_EXPERTS, dtype=jnp.int32)
    token_gates = jnp.sum(
        route_weight.astype(jnp.float32)[:, :, None]
        * (route_member[:, :, None] == member_ids[None, None, :]).astype(jnp.float32),
        axis=1,
    ).astype(jnp.bfloat16)
    send_gates = jnp.dot(placing, token_gates, preferred_element_type=jnp.float32).astype(
        jnp.bfloat16
    )
    send_gates = send_gates.reshape(groups, capacity * GROUP_EXPERTS)
    send_gates = jnp.pad(send_gates, ((0, 0), (0, LANES - capacity * GROUP_EXPERTS)))
    arrived_gates = lax.all_to_all(send_gates, "sp", split_axis=0, concat_axis=0, tiled=True)
    pooled_gates = lax.all_gather(arrived_gates, Z, axis=0, tiled=True)
    flat_gates = (
        pooled_gates[:, : capacity * GROUP_EXPERTS]
        .reshape(depth * slots, GROUP_EXPERTS)
        .astype(jnp.float32)
    )

    def chip_weights(shard, dim):
        return jnp.concatenate([shard, lax.ppermute(shard, CORE, SWAP)], axis=dim)

    gate_chip = chip_weights(gate_weight, 2)
    up_chip = chip_weights(up_weight, 2)
    down_chip = chip_weights(down_weight, 1)
    hid = gate_chip.shape[2]

    send_rows = jnp.dot(placing, normed, preferred_element_type=jnp.float32).astype(jnp.bfloat16)
    arrived = lax.all_to_all(
        send_rows.reshape(groups, capacity * width // LANES, LANES),
        "sp",
        split_axis=0,
        concat_axis=0,
        tiled=True,
    )
    flat_rows = lax.all_gather(arrived.reshape(slots, width), Z, axis=0, tiled=True)
    hidden = []
    for e in range(GROUP_EXPERTS):
        gate_pre = jnp.dot(flat_rows, gate_chip[e], preferred_element_type=jnp.float32)
        up_pre = jnp.dot(flat_rows, up_chip[e], preferred_element_type=jnp.float32)
        gated = jax.nn.silu(gate_pre) * up_pre * flat_gates[:, e : e + 1]
        hidden.append(gated.astype(jnp.bfloat16))
    partial_out = jnp.dot(
        jnp.concatenate(hidden, axis=1),
        down_chip.reshape(GROUP_EXPERTS * hid, width),
        preferred_element_type=jnp.float32,
    ).astype(jnp.bfloat16)
    summed = lax.psum_scatter(partial_out, Z, scatter_dimension=0, tiled=True)
    returned = lax.all_to_all(
        summed.reshape(groups, capacity * width // LANES, LANES),
        "sp",
        split_axis=0,
        concat_axis=0,
        tiled=True,
    )
    expert_out = lax.dot_general(
        placing,
        returned.reshape(slots, width),
        (((0,), (0,)), ((), ())),
        preferred_element_type=jnp.float32,
    )
    return (mixed_float + expert_out).astype(jnp.bfloat16)


def solution(mesh):
    torus = Mesh(mesh.devices.reshape(mesh.shape["sp"], 8, 2), ("sp", Z, CORE))
    placed = (
        P("sp", TP),
        P("sp", None),
        P("sp", None),
        P(TP),
        P(TP, None),
        P(SP_TP, None),
        P(),
        P(),
        P(SP_TP),
        P(SP_TP, None),
        P(SP_TP, None),
        P("sp", None, TP),
        P("sp", None, TP),
        P("sp", TP, None),
    )
    return jax.shard_map(
        per_device, mesh=torus, in_specs=placed, out_specs=P(SP_TP, None), check_vma=False
    )
```

time: 389 us -> 286 us (0.74)
  waiting for transfers between devices: 173 us -> 131 us
  local copies, waits for them, and re-layouts: 59.5 us -> 17.8 us
  blocking collectives: 80.7 us -> 58.9 us
  starting transfers between devices: 13.5 us -> 20.2 us
    reduce_scatter x1, waiting for transfers between devices: 97.8 us -> 64.1 us  [per_device(): summed = lax.psum_scatter(partial_out, Z, scatter_dimension=0, tiled=True)]
    all_to_all x4 -> x2, blocking collectives: 60.1 us -> 36.9 us  [the longest x1 18.8 us: per_device(): lax.all_to_all(send_rows.reshape(groups, capacity * width // LANES, LANES...]
    convert_element_type x3 -> x2, local copies, waits for them, and re-layouts: 18.1 us -> 0.38 us  [the longest x1 0.22 us: per_device(): flat_gates = pooled_gates[:, :capacity * GROUP_EXPERTS].reshape(depth * s...]
    reshape x5, local copies, waits for them, and re-layouts: 20.6 us -> 3.2 us  [the longest x1 1.39 us: per_device(): summed.reshape(groups, capacity * width // LANES, LANES)]
    all_gather x2 -> x0, local copies, waits for them, and re-layouts: 15.6 us -> none  [the longest x1 15.4 us: per_device(): lax.all_gather(arrived_rows, TP, axis=0, tiled=True)]
    all_gather x2, waiting for transfers between devices: 49.1 us -> 38 us  [the longest x1 22.4 us: per_device(): weight_rows = lax.all_gather(out_weight, Z, axis=0, tiled=False)]
    concatenate x0 -> x2, local copies, waits for them, and re-layouts: none -> 5.52 us  [chip_weights(): return jnp.concatenate([shard, lax.ppermute(shard, CORE, SWAP)], axis=dim)]
    unnamed x16 -> x28, local copies, waits for them, and re-layouts: 0.81 us -> 5.06 us
  transfers between devices with their start and end apart: 6 -> 11, of which waited for: 5 -> 7; matrix products, arithmetic and copies ran while one was open for 3% -> 9% of each run, Pallas kernels for 0% -> 0%
where the time goes in v1:
time: 286 us; the launch traced here: 285 us
  waiting for transfers between devices  131 us (46%)
  blocking collectives  58.9 us (21%)
  matrix products  37.4 us (13%)
  starting transfers between devices  20.2 us (7%)
  local copies, waits for them, and re-layouts  17.8 us (6%)
  between operations  14.2 us (5%)
  other arithmetic  5.61 us (2%)
    reduce_scatter x1, waiting for transfers between devices, per_device(): summed = lax.psum_scatter(partial_out, Z, scatter_dimension=0, tiled=True)  64.1 us
    all_to_all x1, waiting for transfers between devices, per_device(): lax.all_to_all(attended.reshape(depth, 2, tok_rows, HEAD_DIM), Z, split_a...  22.7 us
    all_gather x1, waiting for transfers between devices, per_device(): weight_rows = lax.all_gather(out_weight, Z, axis=0, tiled=False)  22.4 us
    all_gather x1, blocking collectives, per_device(): pooled_gates = lax.all_gather(arrived_gates, Z, axis=0, tiled=True)  22 us
    all_to_all x1, blocking collectives, per_device(): lax.all_to_all(send_rows.reshape(groups, capacity * width // LANES, LANES...  18.8 us
    all_to_all x1, blocking collectives, per_device(): lax.all_to_all(summed.reshape(groups, capacity * width // LANES, LANES),...  18.1 us
    all_gather x1, waiting for transfers between devices, per_device(): lax.all_gather(arrived.reshape(slots, width), Z, axis=0, tiled=True)  15.6 us
    dot_general x3, matrix products, per_device(): up_pre = jnp.dot(flat_rows, up_chip[e], preferred_element_type=jnp.float32)  9.4 us
  transfers between devices with their start and end apart: 11, of which 7 were waited for; matrix products, arithmetic and copies ran while one was open for 9% of the time, Pallas kernels for 0%

profile of v1, /device:TPU:1, one launch (start us, length us, event | category | flops | bytes accessed | tf_op | source)
XLA Modules:
  0.0 285.3 jit_solution(4098342262950392075)
XLA Ops:
  6.5 0.7 all-gather.7.cloned.1.call-update
  7.3 1.3 dynamic-slice_bitcast_fusion
  8.6 3.9 %collective-permute-start = (bf16[2,128,128]{2,1,0:T(8,128)(2,1)S(1)}, bf16[2,128,128]{2,1,0:T(8,128)(2,1)S(1)}, u32[]{:S(2)}, u32[]{:S(2)}) collective-permute-start(bf16[2,128,128]{2,1,0:T(8,128)(2,1)S(1)} %get-tuple-element.13), channel_id=1, source_target_pairs={{0,16},{16,32},{32,48},{48,64},{64,80},{80,96},{96,112},{112,128},... | collective-permute-start | bytes 196616 | tf_op jit(solution)/shard_map/ppermute | solution.py:29
  12.5 1.3 collective-permute-start.1
  14.5 0.1 fusion.36
  14.6 0.1 add_add_fusion
  14.7 2.9 %collective-permute-done.1 = bf16[2,128,128]{2,1,0:T(8,128)(2,1)S(1)} collective-permute-done((bf16[2,128,128]{2,1,0:T(8,128)(2,1)S(1)}, bf16[2,128,128]{2,1,0:T(8,128)(2,1)S(1)}, u32[]{:S(2)}, u32[]{:S(2)}) %collective-permute-start.1) | collective-permute-done | bytes 65568 | tf_op jit(solution)/shard_map/ppermute | solution.py:30
  17.5 0.1 pad_maximum_fusion.2
  17.6 0.8 fusion.42
  18.4 0.4 pad_maximum_fusion
  18.8 4.2 %fusion.43 = (f32[16,128]{1,0:T(8,128)S(1)}, f32[16,1,128,384]{2,3,0,1:T(8,128)S(1)}) fusion(bf16[16,128,128]{2,1,0:T(8,128)(2,1)S(1)} %bitcast.90, bf16[2,16,384,128]{3,2,1,0:T(8,128)(2,1)S(1)} %pad_maximum_fusion, pred[16,384]{1,0:T(8,128)(4,1)S(1)} %get-tuple-element.16, pred[16,384]{1,0:T(8,128)(4,1)S(1)} %get-tuple-element.15, ...), kind=kOutput, calls=%fused_computation.94 | convolution fusion | flops 207616000 | bytes 5296128 | tf_op jit(solution)/shard_map/nqhd,nkd->nhqk/dot_general | solution.py:63
  23.0 0.4 fusion.2
  23.4 1.8 fusion.12
  25.3 8.3 %all-to-all-start = ((bf16[8,2,128,128]{2,3,1,0:T(8,128)(2,1)}), bf16[8,2,128,128]{2,3,1,0:T(8,128)(2,1)S(1)}, u32[]{:S(2)}, u32[]{:S(2)}) async-start(bf16[8,2,128,128]{2,3,1,0:T(8,128)(2,1)} %bitcast.12), calls=%async_computation | async-start | bytes 1048576 | tf_op jit(solution)/shard_map/all_to_all | solution.py:103
  33.6 0.0 all-gather.5.cloned.1.call-start
  33.7 22.7 %all-to-all-done = bf16[8,2,128,128]{2,3,1,0:T(8,128)(2,1)S(1)} async-done(((bf16[8,2,128,128]{2,3,1,0:T(8,128)(2,1)}), bf16[8,2,128,128]{2,3,1,0:T(8,128)(2,1)S(1)}, u32[]{:S(2)}, u32[]{:S(2)}) %all-to-all-start) | async-done | bytes 524320 | tf_op jit(solution)/shard_map/all_to_all | solution.py:103
  56.3 22.4 %all-gather.7.cloned.1.call-done = bf16[1024,2048]{1,0:T(8,128)(2,1)} async-done(((bf16[128,2048]{1,0:T(8,128)(2,1)}), bf16[1024,2048]{1,0:T(8,128)(2,1)}) %all-gather.7.cloned.1.call-update) | async-done | bytes 4194320 | tf_op jit(solution)/shard_map/all_gather | solution.py:101
  78.7 2.9 %fusion.3 = bf16[128,2048]{1,0:T(8,128)(2,1)S(1)} fusion(bf16[8,128,2048]{2,1,0:T(8,128)(2,1)} %bitcast.91, bf16[8,2,128,128]{2,3,1,0:T(8,128)(2,1)S(1)} %all-to-all-done, s32[]{:T(128)S(6)} %select_n.24), kind=kOutput, calls=%fused_computation.14 | convolution fusion | flops 537133056 | bytes 4980740 | tf_op jit(solution)/shard_map/zrk,zkn->rn/dot_general | solution.py:109
  81.6 1.0 collective-permute-start.2
  82.6 0.1 fusion.31
  82.7 0.2 reduce_window_sum.11
  82.9 0.2 select_reduce_fusion
  83.1 0.0 copy-start.6
  83.1 1.1 collective-permute-done.2
  84.2 3.0 %multiply_reduce_fusion = (f32[128]{0:T(128)S(1)}, f32[128,2048]{1,0:T(8,128)S(1)}) fusion(bf16[128,2048]{1,0:T(8,128)(2,1)S(1)} %collective-permute-done.2, bf16[8,128,2048]{2,1,0:T(8,128)(2,1)} %bitcast.92, bf16[8,2,128,128]{2,3,1,0:T(8,128)(2,1)S(1)} %all-to-all-done, s32[]{:T(128)S(6)} %select_n.23), kind=kOutput, calls=%fused_computation.49 | convolution fusion | flops 537919360 | bytes 6029828 | tf_op jit(solution)/shard_map/zrk,zkn->rn/dot_general | solution.py:109
  87.2 0.4 fusion.15
  87.7 0.4 convolution_convert_fusion.1
  88.1 0.3 reshape.182
  88.4 18.8 %all_to_all.27 = bf16[16,160,128]{2,1,0:T(8,128)(2,1)S(1)} all-to-all(bf16[16,160,128]{2,1,0:T(8,128)(2,1)S(1)} %reshape.182), channel_id=1, replica_groups=mesh['sp'=16,'tp_0'=8,'tp_1'=2] {'sp'}, dimensions={0} | all-to-all | bytes 1310720 | tf_op jit(solution)/shard_map/all_to_all | solution.py:156
  107.1 1.1 reshape.183
  108.3 0.0 all-gather.5.cloned.1.call-update
  108.3 1.6 collective-permute-start.3
  109.9 0.1 collective-permute-start.4
  110.0 0.4 collective-permute-start.5
  110.4 0.1 convolution_convert_fusion.2
  110.5 0.2 copy.49
  110.7 0.1 reshape.184
  110.8 0.6 copy.50
  111.4 3.5 %all-to-all-start.2 = ((bf16[16,1,128]{2,1,0:T(2,128)(2,1)}), bf16[16,1,128]{2,1,0:T(2,128)(2,1)S(1)}, u32[]{:S(2)}, u32[]{:S(2)}) async-start(bf16[16,1,128]{2,1,0:T(2,128)(2,1)} %copy.50), calls=%async_computation.2 | async-start | bytes 16384 | tf_op jit(solution)/shard_map/all_to_all | solution.py:139
  114.9 0.0 reduce-scatter.2.cloned.1.call-start
  115.0 2.8 constant_dynamic-update-slice_fusion.1
  117.8 1.4 constant_dynamic-update-slice_fusion.3
  119.2 2.0 all-to-all-done.2
  121.2 22.0 %all-gather.1 = bf16[128,1,128]{2,0,1:T(8,128)(2,1)S(1)} all-gather(bf16[16,1,128]{2,0,1:T(8,128)(2,1)S(1)} %copy.51), channel_id=3, replica_groups=mesh['sp'=16,'tp_0'=8,'tp_1'=2] {'tp_0'}, dimensions={0}, use_global_device_ids=true | all-gather | bytes 36864 | tf_op jit(solution)/shard_map/all_gather | solution.py:140
  143.2 0.2 reshape.188
  143.4 0.9 slice_reduce_fusion.2
  144.4 2.8 constant_dynamic-update-slice_fusion
  147.2 2.7 constant_dynamic-update-slice_fusion.2
  149.9 3.6 %pad_maximum_fusion.1 = bf16[3,256,2048]{2,1,0:T(8,128)(2,1)} fusion(bf16[3,128,2048]{2,1,0:T(8,128)(2,1)} %collective-permute-done.5, bf16[3,128,2048]{2,1,0:T(8,128)(2,1)S(1)} %copy-done.4), kind=kLoop, calls=%fused_computation.2 | loop fusion | flops 6291456 | bytes 6291456 | tf_op jit(solution)/shard_map/concatenate | solution.py:148
  153.6 15.6 %all-gather.5.cloned.1.call-done = bf16[1280,2048]{1,0:T(8,128)(2,1)} async-done(((bf16[160,2048]{1,0:T(8,128)(2,1)}), bf16[1280,2048]{1,0:T(8,128)(2,1)}) %all-gather.5.cloned.1.call-update) | async-done | bytes 5242896 | tf_op jit(solution)/shard_map/all_gather | solution.py:163
  169.1 4.5 %fusion.23 = f32[1280,256]{0,1:T(8,128)S(1)} fusion(bf16[1280,2048]{1,0:T(8,128)(2,1)} %all-gather.5.cloned.1.call-done, bf16[3,2048,256]{2,1,0:T(8,128)(2,1)} %constant_dynamic-update-slice_fusion), kind=kOutput, calls=%fused_computation.47 | convolution fusion | flops 1342177280 | bytes 7602176 | tf_op jit(solution)/shard_map/dot_general | solution.py:166
  173.6 0.8 copy-done.11
  174.4 1.7 fusion.21
  176.1 1.7 fusion.19
  177.9 3.1 %multiply_convert_fusion.2 = bf16[1280,256]{0,1:T(8,128)(2,1)S(1)} fusion(f32[1280,256]{0,1:T(8,128)S(1)} %fusion.23, bf16[1280,2048]{1,0:T(8,128)(2,1)S(1)} %copy-done.11, bf16[3,2048,256]{2,1,0:T(8,128)(2,1)} %constant_dynamic-update-slice_fusion.2, f32[1280]{0:T(1024)S(1)} %get-tuple-element.5), kind=kOutput, calls=%fused_computation.29 | convolution fusion | flops 1344471040 | bytes 8262656 | tf_op jit(solution)/shard_map/dot_general | solution.py:167
  181.0 3.1 %multiply_convert_fusion.1 = bf16[1280,256]{0,1:T(8,128)(2,1)S(1)} fusion(f32[1280,256]{0,1:T(8,128)S(1)} %fusion.21, bf16[1280,2048]{1,0:T(8,128)(2,1)S(1)} %copy-done.11, bf16[3,2048,256]{2,1,0:T(8,128)(2,1)} %constant_dynamic-update-slice_fusion.2, f32[1280]{0:T(1024)S(1)} %get-tuple-element.7), kind=kOutput, calls=%fused_computation.28 | convolution fusion | flops 1344471040 | bytes 8262656 | tf_op jit(solution)/shard_map/dot_general | solution.py:167
  184.1 3.2 %multiply_convert_fusion = bf16[1280,256]{0,1:T(8,128)(2,1)S(1)} fusion(f32[1280,256]{0,1:T(8,128)S(1)} %fusion.19, bf16[1280,2048]{1,0:T(8,128)(2,1)S(1)} %copy-done.11, bf16[3,2048,256]{2,1,0:T(8,128)(2,1)} %constant_dynamic-update-slice_fusion.2, f32[1280]{0:T(1024)S(1)} %get-tuple-element.6), kind=kOutput, calls=%fused_computation.27 | convolution fusion | flops 1344471040 | bytes 8262656 | tf_op jit(solution)/shard_map/dot_general | solution.py:167
  187.3 6.4 %convolution_convert_fusion = bf16[1280,2048]{1,0:T(8,128)(2,1)} fusion(bf16[768,2048]{1,0:T(8,128)(2,1)S(1)} %bitcast.94, bf16[1280,256]{0,1:T(8,128)(2,1)S(1)} %multiply_convert_fusion, bf16[1280,256]{0,1:T(8,128)(2,1)S(1)} %multiply_convert_fusion.1, bf16[1280,256]{0,1:T(8,128)(2,1)S(1)} %multiply_convert_fusion.2), kind=kOutput, calls=%fused_computation | convolution fusion | flops 4035051520 | bytes 10354688 | tf_op jit(solution)/shard_map/dot_general | solution.py:170
  193.7 0.0 reduce-scatter.2.cloned.1.call-update
  193.7 64.1 %reduce-scatter.2.cloned.1.call-done = bf16[160,2048]{1,0:T(8,128)(2,1)} async-done(((bf16[1280,2048]{1,0:T(8,128)(2,1)}), bf16[160,2048]{1,0:T(8,128)(2,1)}) %reduce-scatter.2.cloned.1.call-update) | async-done | bytes 655376 | tf_op jit(solution)/shard_map/reduce_scatter | solution.py:175
  257.8 1.4 reshape.186
  259.2 18.1 %all_to_all.28 = bf16[16,160,128]{2,1,0:T(8,128)(2,1)S(1)} all-to-all(bf16[16,160,128]{2,1,0:T(8,128)(2,1)S(1)} %reshape.186), channel_id=1, replica_groups=mesh['sp'=16,'tp_0'=8,'tp_1'=2] {'sp'}, dimensions={0} | all-to-all | bytes 1310720 | tf_op jit(solution)/shard_map/all_to_all | solution.py:176
  277.3 0.3 reshape.187
  277.6 1.1 fusion.4
  (42 shorter events, 0.2 us)
Async XLA Ops:
  6.5 12.3 %copy-start = (bf16[2048,128]{1,0:T(8,128)(2,1)S(1)}, bf16[2048,128]{1,0:T(8,128)(2,1)}, u32[]{:S(2)}) copy-start(bf16[2048,128]{1,0:T(8,128)(2,1)} %param.14) | copy-start | bytes 1572868
  6.5 72.2 %all-gather.7.cloned.1.call-start = ((), (), s32[]{:S(2)}) async-start(), calls=%async_computation.7 | async-start | bytes 4718592 | tf_op jit(solution)/shard_map/all_gather | solution.py:101
  8.6 6.1 %collective-permute-start = (bf16[2,128,128]{2,1,0:T(8,128)(2,1)S(1)}, bf16[2,128,128]{2,1,0:T(8,128)(2,1)S(1)}, u32[]{:S(2)}, u32[]{:S(2)}) collective-permute-start(bf16[2,128,128]{2,1,0:T(8,128)(2,1)S(1)} %get-tuple-element.13), channel_id=1, source_target_pairs={{0,16},{16,32},{32,48},{48,64},{64,80},{80,96},{96,112},{112,128},... | collective-permute-start | bytes 196616 | tf_op jit(solution)/shard_map/ppermute | solution.py:29
  12.5 5.0 %collective-permute-start.1 = (bf16[2,128,128]{2,1,0:T(8,128)(2,1)S(1)}, bf16[2,128,128]{2,1,0:T(8,128)(2,1)S(1)}, u32[]{:S(2)}, u32[]{:S(2)}) collective-permute-start(bf16[2,128,128]{2,1,0:T(8,128)(2,1)S(1)} %get-tuple-element.14), channel_id=1, source_target_pairs={{16,0},{32,16},{48,32},{64,48},{80,64},{96,80},{112,96},{128,112},... | collective-permute-start | bytes 196616 | tf_op jit(solution)/shard_map/ppermute | solution.py:30
  25.3 57.3 %copy-start.9 = (s32[128]{0:T(128)S(1)}, s32[128]{0:T(128)}, u32[]{:S(2)}) copy-start(s32[128]{0:T(128)} %param.22) | copy-start | bytes 1540
  25.3 31.0 %all-to-all-start = ((bf16[8,2,128,128]{2,3,1,0:T(8,128)(2,1)}), bf16[8,2,128,128]{2,3,1,0:T(8,128)(2,1)S(1)}, u32[]{:S(2)}, u32[]{:S(2)}) async-start(bf16[8,2,128,128]{2,3,1,0:T(8,128)(2,1)} %bitcast.12), calls=%async_computation | async-start | bytes 1048576 | tf_op jit(solution)/shard_map/all_to_all | solution.py:103
  33.6 135.5 %all-gather.5.cloned.1.call-start = ((), (), s32[]{:S(2)}) async-start(), calls=%async_computation.5 | async-start | bytes 5898240 | tf_op jit(solution)/shard_map/all_gather | solution.py:163
  81.6 2.5 collective-permute-start.2
  83.1 4.1 %copy-start.6 = (bf16[128,2048]{1,0:T(8,128)(2,1)S(1)}, bf16[128,2048]{1,0:T(8,128)(2,1)}, u32[]{:S(2)}) copy-start(bf16[128,2048]{1,0:T(8,128)(2,1)} %param.19) | copy-start | bytes 1572868
  83.1 4.1 %copy-start.7 = (f32[2048]{0:T(1024)S(1)}, f32[2048]{0:T(1024)}, u32[]{:S(2)}) copy-start(f32[2048]{0:T(1024)} %param.20) | copy-start | bytes 24580
  83.1 4.6 %copy-start.8 = (f32[2048]{0:T(1024)S(1)}, f32[2048]{0:T(1024)}, u32[]{:S(2)}) copy-start(f32[2048]{0:T(1024)} %param.21) | copy-start | bytes 24580
  87.6 22.8 %copy-start.12 = (bf16[128,2]{0,1:T(2,128)(2,1)S(1)}, bf16[128,2]{0,1:T(2,128)(2,1)}, u32[]{:S(2)}) copy-start(bf16[128,2]{0,1:T(2,128)(2,1)} %param.24) | copy-start | bytes 1540
  87.6 22.7 %copy-start.10 = (s32[128,2]{0,1:T(2,128)S(1)}, s32[128,2]{0,1:T(2,128)}, u32[]{:S(2)}) copy-start(s32[128,2]{0,1:T(2,128)} %param.23) | copy-start | bytes 3076
  107.1 10.7 %copy-start.3 = (bf16[3,2048,128]{2,1,0:T(8,128)(2,1)S(1)}, bf16[3,2048,128]{2,1,0:T(8,128)(2,1)}, u32[]{:S(2)}) copy-start(bf16[3,2048,128]{2,1,0:T(8,128)(2,1)} %param.26) | copy-start | bytes 4718596
  108.3 36.1 %collective-permute-start.3 = (bf16[3,2048,128]{2,1,0:T(8,128)(2,1)}, bf16[3,2048,128]{2,1,0:T(8,128)(2,1)}, u32[]{:S(2)}, u32[]{:S(2)}) collective-permute-start(bf16[3,2048,128]{2,1,0:T(8,128)(2,1)} %param.25), channel_id=1, source_target_pairs={{0,1},{1,0},{2,3},{3,2},{4,5},{5,4},{6,7},{7,6},{8,9},{9,8},{10,11... | collective-permute-start | bytes 4718600 | tf_op jit(solution)/shard_map/ppermute | solution.py:148
  109.9 37.4 %collective-permute-start.4 = (bf16[3,2048,128]{2,1,0:T(8,128)(2,1)}, bf16[3,2048,128]{2,1,0:T(8,128)(2,1)}, u32[]{:S(2)}, u32[]{:S(2)}) collective-permute-start(bf16[3,2048,128]{2,1,0:T(8,128)(2,1)} %param.26), channel_id=1, source_target_pairs={{0,1},{1,0},{2,3},{3,2},{4,5},{5,4},{6,7},{7,6},{8,9},{9,8},{10,11... | collective-permute-start | bytes 4718600 | tf_op jit(solution)/shard_map/ppermute | solution.py:148
  110.0 40.0 %collective-permute-start.5 = (bf16[3,128,2048]{2,1,0:T(8,128)(2,1)}, bf16[3,128,2048]{2,1,0:T(8,128)(2,1)}, u32[]{:S(2)}, u32[]{:S(2)}) collective-permute-start(bf16[3,128,2048]{2,1,0:T(8,128)(2,1)} %param.27), channel_id=1, source_target_pairs={{0,1},{1,0},{2,3},{3,2},{4,5},{5,4},{6,7},{7,6},{8,9},{9,8},{10,11... | collective-permute-start | bytes 4718600 | tf_op jit(solution)/shard_map/ppermute | solution.py:148
  111.4 9.8 %all-to-all-start.2 = ((bf16[16,1,128]{2,1,0:T(2,128)(2,1)}), bf16[16,1,128]{2,1,0:T(2,128)(2,1)S(1)}, u32[]{:S(2)}, u32[]{:S(2)}) async-start(bf16[16,1,128]{2,1,0:T(2,128)(2,1)} %copy.50), calls=%async_computation.2 | async-start | bytes 16384 | tf_op jit(solution)/shard_map/all_to_all | solution.py:139
  114.9 142.9 %reduce-scatter.2.cloned.1.call-start = ((), (), s32[]{:S(2)}) async-start(), calls=%async_computation.6 | async-start | bytes 5898240 | tf_op jit(solution)/shard_map/reduce_scatter | solution.py:175
  144.4 5.5 %copy-start.4 = (bf16[3,128,2048]{2,1,0:T(8,128)(2,1)S(1)}, bf16[3,128,2048]{2,1,0:T(8,128)(2,1)}, u32[]{:S(2)}) copy-start(bf16[3,128,2048]{2,1,0:T(8,128)(2,1)} %param.27) | copy-start | bytes 4718596
  169.1 4.5 %copy-start.5 = (bf16[3,2048,256]{2,1,0:T(8,128)(2,1)S(1)}, bf16[3,2048,256]{2,1,0:T(8,128)(2,1)}, u32[]{:S(2)}) copy-start(bf16[3,2048,256]{2,1,0:T(8,128)(2,1)} %constant_dynamic-update-slice_fusion) | copy-start | bytes 9437188
  169.1 5.3 %copy-start.11 = (bf16[1280,2048]{1,0:T(8,128)(2,1)S(1)}, bf16[1280,2048]{1,0:T(8,128)(2,1)}, u32[]{:S(2)}) copy-start(bf16[1280,2048]{1,0:T(8,128)(2,1)} %all-gather.5.cloned.1.call-done) | copy-start | bytes 15728644
  184.1 3.2 %copy-start.2 = (bf16[3,256,2048]{2,1,0:T(8,128)(2,1)S(1)}, bf16[3,256,2048]{2,1,0:T(8,128)(2,1)}, u32[]{:S(2)}) copy-start(bf16[3,256,2048]{2,1,0:T(8,128)(2,1)} %pad_maximum_fusion.1) | copy-start | bytes 9437188
  193.7 85.0 %copy-start.1 = (bf16[2048,128]{1,0:T(8,128)(2,1)S(1)}, bf16[2048,128]{1,0:T(8,128)(2,1)}, u32[]{:S(2)}) copy-start(bf16[2048,128]{1,0:T(8,128)(2,1)} %param.14) | copy-start | bytes 1572868
Sparse Core Ops, SparseCore 0:
  9.1 69.5 all-gather.6
  108.4 60.6 all-gather.4
  193.8 63.9 reduce-scatter.1

commit v2 on v1

v2 whole, which is shorter than its diff:
```python
import jax
import jax.numpy as jnp
from jax import lax
from jax.experimental import pallas as pl
from jax.experimental.pallas import tpu as pltpu
from jax.sharding import Mesh
from jax.sharding import PartitionSpec as P

HEADS = 16
KV_HEADS = 4
HEAD_DIM = 128
WINDOW = 128
BLOCK = 128
GROUP_EXPERTS = 3
GROUP_CAP = 10
LANES = 128
Z = "tp_0"
CORE = "tp_1"
TP = (Z, CORE)
SP_TP = ("sp", Z, CORE)
SWAP = [(0, 1), (1, 0)]

EPS = 1e-06
NEG_BIG = -1e30


def extended(block, width):
    count = lax.axis_size("sp")
    forward = [(i, i + 1) for i in range(count - 1)]
    backward = [(target, source) for source, target in forward]
    low = lax.ppermute(block[:, block.shape[1] - width :], "sp", forward)
    high = lax.ppermute(block[:, :width], "sp", backward)
    return jnp.concatenate([low, block, high], axis=1)


def chip_attention(queries, key_heads, value_heads, sink_logit):
    seq_rows = queries.shape[0]
    core = lax.axis_index(CORE)
    key_start = lax.axis_index(Z) * 2 * KV_HEADS // HEADS * HEAD_DIM
    key_own = lax.dynamic_slice_in_dim(key_heads, key_start, HEAD_DIM, 1)
    value_own = lax.dynamic_slice_in_dim(value_heads, key_start, HEAD_DIM, 1)
    padded = extended(jnp.stack([key_own, value_own]), WINDOW)
    blocks = seq_rows // (2 * BLOCK)
    query_blocks = queries.reshape(blocks, 2, BLOCK, HEAD_DIM)
    query_far = lax.ppermute(
        lax.dynamic_index_in_dim(query_blocks, 1 - core, 1, True), CORE, SWAP
    )
    query_pair = jnp.concatenate(
        [lax.dynamic_index_in_dim(query_blocks, core, 1, True), query_far], axis=1
    )
    sink_pair = jnp.concatenate([sink_logit, lax.ppermute(sink_logit, CORE, SWAP)])
    tile_rows = padded.reshape(2, 2 * blocks + 2, BLOCK, HEAD_DIM)
    key_spans = jnp.concatenate(
        [
            lax.dynamic_slice_in_dim(tile_rows, core + shifted, 2 * blocks - 1, 1)[:, ::2]
            for shifted in range(3)
        ],
        axis=2,
    )
    offset = lax.axis_index("sp") * seq_rows
    seq_total = seq_rows * lax.axis_size("sp")
    block_start = offset + (2 * jnp.arange(blocks, dtype=jnp.int32) + core) * BLOCK
    query_pos = block_start[:, None] + jnp.arange(BLOCK, dtype=jnp.int32)[None, :]
    key_pos = (
        block_start[:, None] + jnp.arange(BLOCK + 2 * WINDOW, dtype=jnp.int32)[None, :] - WINDOW
    )
    inside = (
        (jnp.abs(query_pos[:, :, None] - key_pos[:, None, :]) <= WINDOW)
        & (key_pos >= 0)[:, None, :]
        & (key_pos < seq_total)[:, None, :]
    )
    scores = jnp.einsum(
        "nhqd,nkd->nhqk", query_pair, key_spans[0], preferred_element_type=jnp.float32
    ) * HEAD_DIM ** (-0.5)
    scores = jnp.where(inside[:, None], scores, NEG_BIG)
    sink_col = sink_pair[None, :, None, None]
    row_top = jnp.maximum(jnp.max(scores, axis=3, keepdims=True), sink_col)
    exp_terms = jnp.exp(scores - row_top)
    row_mass = jnp.sum(exp_terms, axis=3, keepdims=True) + jnp.exp(sink_col - row_top)
    weight = (exp_terms / row_mass).astype(jnp.bfloat16)
    return jnp.einsum(
        "nhqk,nkd->nhqd", weight, key_spans[1], preferred_element_type=jnp.float32
    ).astype(jnp.bfloat16)


MAIN_CAP = 7
REL = (0, -1, 1, -2, 2, -3, 3, 4)


def shifts():
    n = lax.axis_size(Z)
    up = [(i, (i + 1) % n) for i in range(n)]
    down = [(i, (i - 1) % n) for i in range(n)]
    return (lambda a: lax.ppermute(a, Z, up)), (lambda a: lax.ppermute(a, Z, down))


def ring_gather(block):
    up, down = shifts()
    half = block.shape[1] // 2
    blocks, low, high = [block], block, block
    for _ in range(3):
        low, high = up(low), down(high)
        blocks += [low, high]
    far = jnp.concatenate([up(low[:, :half]), down(high[:, half:])], axis=1)
    return blocks + [far]


def ring_reduce(parts):
    up, down = shifts()
    half = parts[0].shape[1] // 2
    low, high = up(parts[4][:, :half]), down(parts[4][:, half:])
    low = jnp.concatenate([parts[3][:, :half] + low, parts[3][:, half:]], axis=1)
    high = jnp.concatenate([parts[-3][:, :half], parts[-3][:, half:] + high], axis=1)
    for step in (2, 1):
        low, high = parts[step] + up(low), parts[-step] + down(high)
    return parts[0] + up(low) + down(high)


def in_ring_order(blocks, near_first):
    me = lax.axis_index(Z)
    n = lax.axis_size(Z)
    return [lax.dynamic_index_in_dim(blocks, (me + r) % n, 0, False) for r in near_first]


def experts_kernel(
    rows, gates, gate_own, gate_far, up_own, up_far, down_own, down_far, out, hidden
):
    e = pl.program_id(0)
    total, width = rows.shape
    step = total // (1 + total // 512)
    hid = 2 * gate_own.shape[2]
    wide = 512

    @pl.loop(0, total // step)
    def _(i):
        at = pl.ds(pl.multiple_of(i * step, 16), step)

        for k in range(GROUP_EXPERTS):

            @pl.when(e == k)
            def _():
                weights = jnp.concatenate(
                    [gate_own[0], gate_far[0], up_own[0], up_far[0]], axis=1
                )
                both = jnp.dot(rows[at, :], weights, preferred_element_type=jnp.float32)
                pre = both[:, :hid]
                gated = pre / (1.0 + jnp.exp(-pre)) * both[:, hid:] * gates[0, at, :]
                hidden[at, k * hid : (k + 1) * hid] = gated.astype(jnp.bfloat16)

        @pl.when(e == GROUP_EXPERTS)
        def _():
            pieces = []
            for k in range(GROUP_EXPERTS):
                pieces += [down_own[k], down_far[k]]
            for c in range(0, width, wide):
                cols = slice(c, c + wide)
                down = jnp.concatenate([p[:, cols] for p in pieces], axis=0)
                out[at, cols] = jnp.dot(
                    hidden[at, :], down, preferred_element_type=jnp.float32
                ).astype(jnp.bfloat16)


def experts(rows, gates, gate_pair, up_pair, down_pair):
    total, width = rows.shape
    hid = gate_pair[0].shape[2]
    last = GROUP_EXPERTS - 1
    into = pl.BlockSpec((1, width, hid), lambda e: (jnp.minimum(e, last), 0, 0))
    outof = pl.BlockSpec(
        (GROUP_EXPERTS, hid, width), lambda e: (0, 0, 0), pipeline_mode=pl.Buffered(1)
    )
    whole = pl.BlockSpec((total, width), lambda e: (0, 0), pipeline_mode=pl.Buffered(1))
    work = total * width * hid * 2 * GROUP_EXPERTS
    return pl.pallas_call(
        experts_kernel,
        grid=(GROUP_EXPERTS + 1,),
        in_specs=[
            whole,
            pl.BlockSpec((1, total, 1), lambda e: (jnp.minimum(e, last), 0, 0)),
            into,
            into,
            into,
            into,
            outof,
            outof,
        ],
        out_specs=pl.BlockSpec((total, width), lambda e: (0, 0)),
        out_shape=jax.ShapeDtypeStruct((total, width), jnp.bfloat16),
        scratch_shapes=[pltpu.VMEM((total, GROUP_EXPERTS * 2 * hid), jnp.bfloat16)],
        compiler_params=pltpu.CompilerParams(
            dimension_semantics=("arbitrary",), vmem_limit_bytes=48 * 2**20
        ),
        cost_estimate=pl.CostEstimate(
            flops=6 * work, bytes_accessed=20 * 2**20, transcendentals=total * hid * 6
        ),
        name="experts",
    )(rows, gates.T[:, :, None], *gate_pair, *up_pair, *down_pair)


def per_device(
    queries,
    key_heads,
    value_heads,
    sink_logit,
    out_weight,
    residual,
    mixer_gain,
    expert_gain,
    route_group,
    route_member,
    route_weight,
    gate_weight,
    up_weight,
    down_weight,
):
    depth = lax.axis_size(Z)
    groups = lax.axis_size("sp")
    width = residual.shape[1]
    capacity = GROUP_CAP
    slots = groups * capacity
    cap_a = MAIN_CAP
    cap_b = capacity - cap_a
    slots_a, slots_b = groups * cap_a, groups * cap_b


    gate_pair, up_pair, down_pair = (
        (shard, lax.ppermute(shard, CORE, SWAP))
        for shard in (gate_weight, up_weight, down_weight)
    )

    group_ids = jnp.arange(groups, dtype=jnp.int32)
    chosen = (route_group[:, None] == group_ids[None, :]).astype(jnp.int32)
    group_rank = jnp.sum(chosen * (jnp.cumsum(chosen, axis=0) - 1), axis=1)
    slot_ids = route_group * capacity + group_rank
    placing = (jnp.arange(slots, dtype=jnp.int32)[:, None] == slot_ids[None, :]).astype(
        jnp.bfloat16
    )
    member_ids = jnp.arange(GROUP_EXPERTS, dtype=jnp.int32)
    token_gates = jnp.sum(
        route_weight.astype(jnp.float32)[:, :, None]
        * (route_member[:, :, None] == member_ids[None, None, :]).astype(jnp.float32),
        axis=1,
    ).astype(jnp.bfloat16)
    send_gates = jnp.dot(placing, token_gates, preferred_element_type=jnp.float32).astype(
        jnp.bfloat16
    )
    gate_cols = capacity * GROUP_EXPERTS
    send_gates = jnp.pad(
        send_gates.reshape(groups, gate_cols), ((0, 0), (0, LANES - gate_cols))
    )

    weight_pair = jnp.stack([out_weight, lax.ppermute(out_weight, CORE, SWAP)])
    attended = chip_attention(queries, key_heads, value_heads, sink_logit)
    head_part = jnp.einsum(
        "nhqd,hdm->nqm", attended, weight_pair, preferred_element_type=jnp.float32
    ).astype(jnp.bfloat16)
    projected = lax.psum_scatter(
        head_part.reshape(-1, width), Z, scatter_dimension=0, tiled=True
    ).astype(jnp.float32)

    send_gates, head_part = lax.optimization_barrier((send_gates, head_part))
    arrived_gates = lax.all_to_all(send_gates, "sp", split_axis=0, concat_axis=0, tiled=True)
    pooled_gates = lax.all_to_all(
        jnp.broadcast_to(arrived_gates[None], (depth, groups, LANES)),
        Z,
        split_axis=0,
        concat_axis=0,
        tiled=True,
    )
    pooled_gates = pooled_gates[:, :, :gate_cols].astype(jnp.float32)
    pooled_gates = pooled_gates.reshape(depth, groups, capacity, GROUP_EXPERTS)
    gates_a = pooled_gates[:, :, :cap_a].reshape(depth * slots_a, GROUP_EXPERTS)
    gates_b = pooled_gates[:, :, cap_a:].reshape(depth, slots_b, GROUP_EXPERTS)
    gates_b = jnp.concatenate(in_ring_order(gates_b, REL), axis=0)
    projected, gate_pair, up_pair, down_pair, gates_a, gates_b = lax.optimization_barrier(
        (projected, gate_pair, up_pair, down_pair, gates_a, gates_b)
    )

    proj_scale = lax.rsqrt(jnp.mean(projected * projected, axis=1, keepdims=True) + EPS)
    mixed_rows = (residual.astype(jnp.float32) + mixer_gain * (projected * proj_scale)).astype(
        jnp.bfloat16
    )
    mixed_float = mixed_rows.astype(jnp.float32)
    norm_scale = lax.rsqrt(jnp.mean(mixed_float * mixed_float, axis=1, keepdims=True) + EPS)
    normed = (mixed_float * norm_scale * expert_gain).astype(jnp.bfloat16)

    def exchange(rows):
        return lax.all_to_all(
            rows.reshape(groups, -1, LANES), "sp", split_axis=0, concat_axis=0, tiled=True
        )

    send_rows = jnp.dot(placing, normed, preferred_element_type=jnp.float32).astype(jnp.bfloat16)
    arrived = exchange(send_rows)
    cut = cap_a * width // LANES
    pool_a = lax.all_gather(arrived[:, :cut].reshape(slots_a, width), Z, axis=0, tiled=True)
    pool_b = ring_gather(arrived[:, cut:].reshape(slots_b, width))

    part_b = experts(jnp.concatenate(pool_b, axis=0), gates_b, gate_pair, up_pair, down_pair)
    pool_a, part_b = lax.optimization_barrier((pool_a, part_b))
    part_a = experts(pool_a, gates_a, gate_pair, up_pair, down_pair)
    sum_a = lax.psum_scatter(part_a, Z, scatter_dimension=0, tiled=True)
    sum_b = ring_reduce(
        {r: part_b[k * slots_b : (k + 1) * slots_b] for k, r in enumerate(REL)}
    )
    back_b = exchange(sum_b)
    back_a = exchange(sum_a)
    returned = jnp.concatenate([back_a, back_b], axis=1).reshape(slots, width)
    expert_out = lax.dot_general(
        placing,
        returned,
        (((0,), (0,)), ((), ())),
        preferred_element_type=jnp.float32,
    )
    return (mixed_float + expert_out).astype(jnp.bfloat16)


def solution(mesh):
    torus = Mesh(mesh.devices.reshape(mesh.shape["sp"], 8, 2), ("sp", Z, CORE))
    placed = (
        P("sp", TP),
        P("sp", None),
        P("sp", None),
        P(TP),
        P(TP, None),
        P(SP_TP, None),
        P(),
        P(),
        P(SP_TP),
        P(SP_TP, None),
        P(SP_TP, None),
        P("sp", None, TP),
        P("sp", None, TP),
        P("sp", TP, None),
    )
    return jax.shard_map(
        per_device, mesh=torus, in_specs=placed, out_specs=P(SP_TP, None), check_vma=False
    )
```

time: 286 us -> 271 us (0.948)
  matrix products: 37.4 us -> 8.59 us
  Pallas kernels: 0 us -> 22.9 us
  starting transfers between devices: 20.2 us -> 42.1 us
  waiting for transfers between devices: 131 us -> 113 us
  blocking collectives: 58.9 us -> 44.8 us
    ppermute x4 -> x22, waiting for transfers between devices: 1.06 us -> 60.4 us  [the longest x8 38.2 us: shifts(): lax.ppermute(a, Z, down)]
    dot_general x12 -> x3, matrix products: 36.8 us -> 8.04 us  [the longest x1 5.09 us: per_device(): jnp.einsum('nhqd,hdm->nqm', attended, weight_pair, preferred_element_type...]
    all_gather x2 -> x1, waiting for transfers between devices: 38 us -> 9.43 us  [per_device(): lax.all_gather(arrived[:, :cut].reshape(slots_a, width), Z, axis=0, tiled...]
    reduce_scatter x1 -> x2, waiting for transfers between devices: 64.1 us -> 36 us  [the longest x1 24.2 us: per_device(): lax.psum_scatter(head_part.reshape(-1, width), Z, scatter_dimension=0, ti...]
    pallas_call x0 -> x2, Pallas kernels: none -> 22.9 us  [experts(): pl.pallas_call(experts_kernel, grid=(GROUP_EXPERTS + 1,), in_specs=[whole...]
    all_gather x1 -> x0, blocking collectives: 22 us -> none  [per_device(): pooled_gates = lax.all_gather(arrived_gates, Z, axis=0, tiled=True)]
    ppermute x4 -> x22, starting transfers between devices: 3.05 us -> 24.2 us  [the longest x8 15.7 us: shifts(): lax.ppermute(a, Z, down)]
    all_to_all x2, waiting for transfers between devices: 24.7 us -> 7.22 us  [the longest x1 7.21 us: per_device(): lax.all_to_all(jnp.broadcast_to(arrived_gates[None], (depth, groups, LANE...]
  transfers between devices with their start and end apart: 11 -> 29, of which waited for: 7 -> 18; matrix products, arithmetic and copies ran while one was open for 9% -> 5% of each run, Pallas kernels for 0% -> 3%
where the time goes in v2:
time: 271 us; the launch traced here: 268 us
  waiting for transfers between devices  113 us (42%)
  blocking collectives  44.8 us (17%)
  starting transfers between devices  42.1 us (16%)
  Pallas kernels  22.9 us (8%)
  local copies, waits for them, and re-layouts  16.1 us (6%)
  between operations  14.5 us (5%)
  matrix products  8.59 us (3%)
  other arithmetic  5.6 us (2%)
    ppermute x8, waiting for transfers between devices, shifts(): lax.ppermute(a, Z, down)  38.2 us
    all_to_all x2, blocking collectives, exchange(): lax.all_to_all(rows.reshape(groups, -1, LANES), 'sp', split_axis=0, conca...  31.6 us
    reduce_scatter x1, waiting for transfers between devices, per_device(): lax.psum_scatter(head_part.reshape(-1, width), Z, scatter_dimension=0, ti...  24.2 us
    pallas_call x2, Pallas kernels, experts(): pl.pallas_call(experts_kernel, grid=(GROUP_EXPERTS + 1,), in_specs=[whole...  22.9 us
    ppermute x8, waiting for transfers between devices, shifts(): lax.ppermute(a, Z, up)  22.2 us
    ppermute x8, starting transfers between devices, shifts(): lax.ppermute(a, Z, down)  15.7 us
    all_to_all x1, blocking collectives, per_device(): lax.all_to_all(send_gates, 'sp', split_axis=0, concat_axis=0, tiled=True)  13.1 us
    reduce_scatter x1, waiting for transfers between devices, per_device(): sum_a = lax.psum_scatter(part_a, Z, scatter_dimension=0, tiled=True)  11.8 us
  transfers between devices with their start and end apart: 29, of which 18 were waited for; matrix products, arithmetic and copies ran while one was open for 5% of the time, Pallas kernels for 3%

profile of v2, /device:TPU:1, one launch (start us, length us, event | category | flops | bytes accessed | tf_op | source)
XLA Modules:
  0.0 267.8 jit_solution(16135570770399607897)
XLA Ops:
  6.5 1.3 dynamic-slice_bitcast_fusion
  7.9 1.3 collective-permute-start.2
  9.2 4.6 %collective-permute-start.1 = (bf16[2,128,128]{2,1,0:T(8,128)(2,1)S(1)}, bf16[2,128,128]{2,1,0:T(8,128)(2,1)S(1)}, u32[]{:S(2)}, u32[]{:S(2)}) collective-permute-start(bf16[2,128,128]{2,1,0:T(8,128)(2,1)S(1)} %get-tuple-element.48), channel_id=1, source_target_pairs={{0,16},{16,32},{32,48},{48,64},{64,80},{80,96},{96,112},{112,128},... | collective-permute-start | bytes 196616 | tf_op jit(solution)/shard_map/ppermute | solution.py:31
  13.8 0.8 constant_dynamic-slice_fusion.4
  14.5 3.2 %collective-permute-start = (bf16[8,1,128,128]{3,2,1,0:T(8,128)(2,1)S(1)}, bf16[8,1,128,128]{3,2,1,0:T(8,128)(2,1)S(1)}, u32[]{:S(2)}, u32[]{:S(2)}) collective-permute-start(bf16[8,1,128,128]{3,2,1,0:T(8,128)(2,1)S(1)} %get-tuple-element.51), channel_id=1, source_target_pairs={{0,1},{1,0},{2,3},{3,2},{4,5},{5,4},{6,7},{7,6},{8,9},{9,8},{10,11... | collective-permute-start | bytes 786440 | tf_op jit(solution)/shard_map/ppermute | solution.py:45
  17.7 0.5 collective-permute-start.4
  19.1 0.6 fusion.4
  19.8 0.7 pad_maximum_fusion.7
  20.6 0.4 constant_dynamic-slice_fusion.2
  21.3 0.7 copy-done.18
  22.0 1.8 fusion
  23.9 1.2 fusion.2
  25.2 5.1 %bitcast_convert_fusion = bf16[8,128,2048]{2,1,0:T(8,128)(2,1)} fusion(f32[8,2,128,384]{3,2,1,0:T(8,128)S(1)} %get-tuple-element.55, f32[8,2,128]{2,1,0:T(2,128)S(1)} %exponential_add_fusion, f32[8,2,128]{2,1,0:T(2,128)S(1)} %broadcast_maximum_fusion, pred[8,128,384]{2,1,0:T(8,128)(4,1)S(1)} %fusion.4, bf16[1,128,2048]{2,1,0:T(8,128)(2,1)} %bitcast.11, ...), kind=kOutput, calls=%fused_computation | convolution fusion | flops 1281884160 | bytes 9584640 | tf_op jit(solution)/shard_map/nhqd,hdm->nqm/dot_general | solution.py:253
  30.4 1.4 copy-done
  31.7 0.5 copy-done.3
  32.2 0.5 collective-permute-start.7
  33.6 13.1 %all_to_all.29 = bf16[16,1,128]{2,1,0:T(2,128)(2,1)S(1)} all-to-all(bf16[16,1,128]{2,1,0:T(2,128)(2,1)S(1)} %copy.60), channel_id=1, replica_groups=mesh['sp'=16,'tp_0'=8,'tp_1'=2] {'sp'}, dimensions={0} | all-to-all | bytes 8192 | tf_op jit(solution)/shard_map/all_to_all | solution.py:261
  46.8 0.6 broadcast_in_dim.19
  47.4 8.2 %all-to-all-start.1 = ((bf16[8,16,128]{2,1,0:T(8,128)(2,1)}), bf16[8,16,128]{2,1,0:T(8,128)(2,1)S(1)}, u32[]{:S(2)}, u32[]{:S(2)}) async-start(bf16[8,16,128]{2,1,0:T(8,128)(2,1)} %broadcast_in_dim.19), calls=%async_computation.2 | async-start | bytes 65536 | tf_op jit(solution)/shard_map/all_to_all | solution.py:262
  55.8 7.2 %all-to-all-done.1 = bf16[8,16,128]{2,1,0:T(8,128)(2,1)S(1)} async-done(((bf16[8,16,128]{2,1,0:T(8,128)(2,1)}), bf16[8,16,128]{2,1,0:T(8,128)(2,1)S(1)}, u32[]{:S(2)}, u32[]{:S(2)}) %all-to-all-start.1) | async-done | bytes 32800 | tf_op jit(solution)/shard_map/all_to_all | solution.py:262
  63.7 0.4 dynamic-slice_reduce_fusion
  64.2 0.7 concatenate.34
  64.9 24.2 %reduce-scatter.3.cloned.1.call-done = bf16[128,2048]{1,0:T(8,128)(2,1)} async-done(((bf16[1024,2048]{1,0:T(8,128)(2,1)}), bf16[128,2048]{1,0:T(8,128)(2,1)}) %reduce-scatter.3.cloned.1.call-update) | async-done | bytes 524304 | tf_op jit(solution)/shard_map/reduce_scatter | solution.py:256
  89.1 1.2 convert_element_type.51
  90.9 0.8 copy-done.5
  91.7 0.4 convolution_convert_fusion
  92.4 18.1 %all_to_all.30 = bf16[16,160,128]{2,1,0:T(8,128)(2,1)S(1)} all-to-all(bf16[16,160,128]{2,1,0:T(8,128)(2,1)S(1)} %reshape.175), channel_id=1, replica_groups=mesh['sp'=16,'tp_0'=8,'tp_1'=2] {'sp'}, dimensions={0} | all-to-all | bytes 1310720 | tf_op jit(solution)/shard_map/all_to_all | solution.py:287
  110.6 1.0 reshape.176
  112.1 0.5 copy.65.gates
  112.7 2.7 collective-permute-start.9
  115.4 3.0 %collective-permute-done.8 = bf16[48,2048]{1,0:T(8,128)(2,1)S(1)} collective-permute-done((bf16[48,2048]{1,0:T(8,128)(2,1)S(1)}, bf16[48,2048]{1,0:T(8,128)(2,1)S(1)}, u32[]{:S(2)}, u32[]{:S(2)}) %collective-permute-start.8) | collective-permute-done | bytes 196640 | tf_op jit(solution)/shard_map/ppermute | solution.py:94
  118.5 2.7 collective-permute-start.11
  121.2 5.8 %collective-permute-done.10 = bf16[48,2048]{1,0:T(8,128)(2,1)S(1)} collective-permute-done((bf16[48,2048]{1,0:T(8,128)(2,1)S(1)}, bf16[48,2048]{1,0:T(8,128)(2,1)S(1)}, u32[]{:S(2)}, u32[]{:S(2)}) %collective-permute-start.10) | collective-permute-done | bytes 196640 | tf_op jit(solution)/shard_map/ppermute | solution.py:94
  126.9 1.6 collective-permute-done.11
  128.5 3.5 %collective-permute-start.13 = (bf16[48,2048]{1,0:T(8,128)(2,1)S(1)}, bf16[48,2048]{1,0:T(8,128)(2,1)S(1)}, u32[]{:S(2)}, u32[]{:S(2)}) collective-permute-start(bf16[48,2048]{1,0:T(8,128)(2,1)S(1)} %collective-permute-done.11), channel_id=1, source_target_pairs={{0,14},{2,0},{4,2},{6,4},{8,6},{10,8},{12,10},{14,12},{1,15},{3,1}... | collective-permute-start | bytes 589832 | tf_op jit(solution)/shard_map/ppermute | solution.py:94
  132.1 7.6 %collective-permute-done.13 = bf16[48,2048]{1,0:T(8,128)(2,1)S(1)} collective-permute-done((bf16[48,2048]{1,0:T(8,128)(2,1)S(1)}, bf16[48,2048]{1,0:T(8,128)(2,1)S(1)}, u32[]{:S(2)}, u32[]{:S(2)}) %collective-permute-start.13) | collective-permute-done | bytes 196640 | tf_op jit(solution)/shard_map/ppermute | solution.py:94
  139.7 3.6 %collective-permute-start.15 = (bf16[48,1024]{1,0:T(8,128)(2,1)S(1)}, bf16[48,1024]{1,0:T(8,128)(2,1)S(1)}, u32[]{:S(2)}, u32[]{:S(2)}) collective-permute-start(bf16[48,1024]{1,0:T(8,128)(2,1)S(1)} %slice.117), channel_id=1, source_target_pairs={{0,14},{2,0},{4,2},{6,4},{8,6},{10,8},{12,10},{14,12},{1,15},{3,1}... | collective-permute-start | bytes 294920 | tf_op jit(solution)/shard_map/ppermute | solution.py:94
  143.5 4.6 %collective-permute-done.15 = bf16[48,1024]{1,0:T(8,128)(2,1)S(1)} collective-permute-done((bf16[48,1024]{1,0:T(8,128)(2,1)S(1)}, bf16[48,1024]{1,0:T(8,128)(2,1)S(1)}, u32[]{:S(2)}, u32[]{:S(2)}) %collective-permute-start.15) | collective-permute-done | bytes 98336 | tf_op jit(solution)/shard_map/ppermute | solution.py:94
  148.1 2.7 %collective-permute-done.14 = bf16[48,1024]{1,0:T(8,128)(2,1)S(1)} collective-permute-done((bf16[48,1024]{1,0:T(8,128)(2,1)S(1)}, bf16[48,1024]{1,0:T(8,128)(2,1)S(1)}, u32[]{:S(2)}, u32[]{:S(2)}) %collective-permute-start.14) | collective-permute-done | bytes 98336 | tf_op jit(solution)/shard_map/ppermute | solution.py:94
  150.8 7.5 %experts.2 = bf16[384,2048]{1,0:T(8,128)(2,1)S(1)} custom-call(bf16[384,2048]{1,0:T(8,128)(2,1)S(1)} %maximum_dynamic-update-slice_fusion.rows, f32[3,384,1]{2,1,0:T(8,128)S(1)} %copy.64.gates, bf16[3,2048,128]{2,1,0:T(8,128)(2,1)S(1)} %copy-done.1, bf16[3,2048,128]{2,1,0:T(8,128)(2,1)} %collective-permute-done.5.gate_far, bf16[3,2048,128]{2,1,0:T(8,128)(2,1)} %up_own.1, ...), custom_call_target="tpu_custom_call" | custom-call | flops 3623878656 | bytes 20971520 | tf_op jit(solution)/shard_map/experts/pallas_call | solution.py:173
  158.3 9.4 %all-gather.2.cloned.1.call-done.rows = bf16[896,2048]{1,0:T(8,128)(2,1)} async-done(((bf16[112,2048]{1,0:T(8,128)(2,1)}), bf16[896,2048]{1,0:T(8,128)(2,1)}) %all-gather.2.cloned.1.call-update) | async-done | bytes 3670032 | tf_op jit(solution)/shard_map/all_gather | solution.py:294
  167.7 1.4 copy-done.2
  169.1 1.4 copy-done.4
  170.5 15.4 %experts.3 = bf16[896,2048]{1,0:T(8,128)(2,1)} custom-call(bf16[896,2048]{1,0:T(8,128)(2,1)} %all-gather.2.cloned.1.call-done.rows, f32[3,896,1]{2,1,0:T(8,128)S(1)} %copy.65.gates, bf16[3,2048,128]{2,1,0:T(8,128)(2,1)S(1)} %copy-done.2, bf16[3,2048,128]{2,1,0:T(8,128)(2,1)} %collective-permute-done.5.gate_far, bf16[3,2048,128]{2,1,0:T(8,128)(2,1)S(1)} %copy-done.4, ...), custom_call_target="tpu_custom_call" | custom-call | flops 8455716864 | bytes 20971520 | tf_op jit(solution)/shard_map/experts/pallas_call | solution.py:173
  186.1 4.7 %collective-permute-done.16 = bf16[48,1024]{1,0:T(8,128)(2,1)S(1)} collective-permute-done((bf16[48,1024]{1,0:T(8,128)(2,1)S(1)}, bf16[48,1024]{1,0:T(8,128)(2,1)S(1)}, u32[]{:S(2)}, u32[]{:S(2)}) %collective-permute-start.16) | collective-permute-done | bytes 98336 | tf_op jit(solution)/shard_map/ppermute | solution.py:94
  190.8 0.4 collective-permute-start.20
  191.2 1.2 collective-permute-start.17
  192.4 1.9 collective-permute-done.20
  194.3 1.6 collective-permute-start.21
  195.9 1.0 collective-permute-done.17
  197.0 1.3 collective-permute-start.18
  198.3 5.8 %collective-permute-done.21 = bf16[48,2048]{1,0:T(8,128)(2,1)S(1)} collective-permute-done((bf16[48,2048]{1,0:T(8,128)(2,1)S(1)}, bf16[48,2048]{1,0:T(8,128)(2,1)S(1)}, u32[]{:S(2)}, u32[]{:S(2)}) %collective-permute-start.21) | collective-permute-done | bytes 196640 | tf_op jit(solution)/shard_map/ppermute | solution.py:94
  204.2 4.0 %collective-permute-done.18 = bf16[48,2048]{1,0:T(8,128)(2,1)S(1)} collective-permute-done((bf16[48,2048]{1,0:T(8,128)(2,1)S(1)}, bf16[48,2048]{1,0:T(8,128)(2,1)S(1)}, u32[]{:S(2)}, u32[]{:S(2)}) %collective-permute-start.18) | collective-permute-done | bytes 196640 | tf_op jit(solution)/shard_map/ppermute | solution.py:94
  208.4 1.5 collective-permute-start.19
  209.8 7.8 %collective-permute-done.22 = bf16[48,2048]{1,0:T(8,128)(2,1)S(1)} collective-permute-done((bf16[48,2048]{1,0:T(8,128)(2,1)S(1)}, bf16[48,2048]{1,0:T(8,128)(2,1)S(1)}, u32[]{:S(2)}, u32[]{:S(2)}) %collective-permute-start.22) | collective-permute-done | bytes 196640 | tf_op jit(solution)/shard_map/ppermute | solution.py:94
  217.6 1.2 collective-permute-start.23
  218.8 1.0 collective-permute-done.19
  219.8 8.9 %collective-permute-done.23 = bf16[48,2048]{1,0:T(8,128)(2,1)S(1)} collective-permute-done((bf16[48,2048]{1,0:T(8,128)(2,1)S(1)}, bf16[48,2048]{1,0:T(8,128)(2,1)S(1)}, u32[]{:S(2)}, u32[]{:S(2)}) %collective-permute-start.23) | collective-permute-done | bytes 196640 | tf_op jit(solution)/shard_map/ppermute | solution.py:94
  228.8 0.8 reshape.179
  229.5 3.6 %all-to-all-start.4 = ((bf16[16,48,128]{2,1,0:T(8,128)(2,1)}), bf16[16,48,128]{2,1,0:T(8,128)(2,1)S(1)}, u32[]{:S(2)}, u32[]{:S(2)}) async-start(bf16[16,48,128]{2,1,0:T(8,128)(2,1)} %reshape.179), calls=%async_computation.6 | async-start | bytes 393216 | tf_op jit(solution)/shard_map/all_to_all | solution.py:287
  233.2 11.8 %reduce-scatter.5.cloned.1.call-done = bf16[112,2048]{1,0:T(8,128)(2,1)} async-done(((bf16[896,2048]{1,0:T(8,128)(2,1)}), bf16[112,2048]{1,0:T(8,128)(2,1)}) %reduce-scatter.5.cloned.1.call-update) | async-done | bytes 458768 | tf_op jit(solution)/shard_map/reduce_scatter | solution.py:300
  245.0 1.2 reshape.178
  246.2 13.5 %all_to_all.31 = bf16[16,112,128]{2,1,0:T(8,128)(2,1)S(1)} all-to-all(bf16[16,112,128]{2,1,0:T(8,128)(2,1)S(1)} %reshape.178), channel_id=1, replica_groups=mesh['sp'=16,'tp_0'=8,'tp_1'=2] {'sp'}, dimensions={0} | all-to-all | bytes 917504 | tf_op jit(solution)/shard_map/all_to_all | solution.py:287
  260.1 1.1 fusion.1
  (121 shorter events, 5.1 us)
Async XLA Ops:
  6.5 82.5 %reduce-scatter.3.cloned.1.call-start = ((), (), s32[]{:S(2)}) async-start(), calls=%async_computation.7 | async-start | bytes 4718592 | tf_op jit(solution)/shard_map/reduce_scatter | solution.py:256
  6.5 7.2 %copy-start.8 = (bf16[2048,128]{1,0:T(8,128)(2,1)S(1)}, bf16[2048,128]{1,0:T(8,128)(2,1)}, u32[]{:S(2)}) copy-start(bf16[2048,128]{1,0:T(8,128)(2,1)} %param.14) | copy-start | bytes 1572868
  7.9 12.6 %collective-permute-start.2 = (bf16[2,128,128]{2,1,0:T(8,128)(2,1)S(1)}, bf16[2,128,128]{2,1,0:T(8,128)(2,1)S(1)}, u32[]{:S(2)}, u32[]{:S(2)}) collective-permute-start(bf16[2,128,128]{2,1,0:T(8,128)(2,1)S(1)} %get-tuple-element.49), channel_id=1, source_target_pairs={{16,0},{32,16},{48,32},{64,48},{80,64},{96,80},{112,96},{128,112},... | collective-permute-start | bytes 196616 | tf_op jit(solution)/shard_map/ppermute | solution.py:32
  9.2 11.3 %collective-permute-start.1 = (bf16[2,128,128]{2,1,0:T(8,128)(2,1)S(1)}, bf16[2,128,128]{2,1,0:T(8,128)(2,1)S(1)}, u32[]{:S(2)}, u32[]{:S(2)}) collective-permute-start(bf16[2,128,128]{2,1,0:T(8,128)(2,1)S(1)} %get-tuple-element.48), channel_id=1, source_target_pairs={{0,16},{16,32},{32,48},{48,64},{64,80},{80,96},{96,112},{112,128},... | collective-permute-start | bytes 196616 | tf_op jit(solution)/shard_map/ppermute | solution.py:31
  14.5 6.7 %collective-permute-start = (bf16[8,1,128,128]{3,2,1,0:T(8,128)(2,1)S(1)}, bf16[8,1,128,128]{3,2,1,0:T(8,128)(2,1)S(1)}, u32[]{:S(2)}, u32[]{:S(2)}) collective-permute-start(bf16[8,1,128,128]{3,2,1,0:T(8,128)(2,1)S(1)} %get-tuple-element.51), channel_id=1, source_target_pairs={{0,1},{1,0},{2,3},{3,2},{4,5},{5,4},{6,7},{7,6},{8,9},{9,8},{10,11... | collective-permute-start | bytes 786440 | tf_op jit(solution)/shard_map/ppermute | solution.py:45
  17.7 2.0 collective-permute-start.3
  17.7 7.5 %collective-permute-start.4 = (bf16[128,2048]{1,0:T(8,128)(2,1)}, bf16[128,2048]{1,0:T(8,128)(2,1)}, u32[]{:S(2)}, u32[]{:S(2)}) collective-permute-start(bf16[128,2048]{1,0:T(8,128)(2,1)} %param.18), channel_id=1, source_target_pairs={{0,1},{1,0},{2,3},{3,2},{4,5},{5,4},{6,7},{7,6},{8,9},{9,8},{10,11... | collective-permute-start | bytes 1572872 | tf_op jit(solution)/shard_map/ppermute | solution.py:251
  21.1 1.0 copy-start.10
  21.2 2.6 copy-start.7
  21.3 0.7 copy-start.18
  30.3 1.4 copy-start
  30.3 1.9 copy-start.3
  30.3 2.4 copy-start.16
  30.3 2.6 copy-start.19
  30.3 2.6 copy-start.17
  31.7 58.6 %collective-permute-start.5 = (bf16[3,2048,128]{2,1,0:T(8,128)(2,1)S(1)}, bf16[3,2048,128]{2,1,0:T(8,128)(2,1)}, u32[]{:S(2)}, u32[]{:S(2)}) collective-permute-start(bf16[3,2048,128]{2,1,0:T(8,128)(2,1)S(1)} %copy-done), channel_id=1, source_target_pairs={{0,1},{1,0},{2,3},{3,2},{4,5},{5,4},{6,7},{7,6},{8,9},{9,8},{10,11... | collective-permute-start | bytes 4718600 | tf_op jit(solution)/shard_map/ppermute | solution.py:226
  32.2 58.1 %collective-permute-start.6 = (bf16[3,2048,128]{2,1,0:T(8,128)(2,1)S(1)}, bf16[3,2048,128]{2,1,0:T(8,128)(2,1)}, u32[]{:S(2)}, u32[]{:S(2)}) collective-permute-start(bf16[3,2048,128]{2,1,0:T(8,128)(2,1)S(1)} %copy-done.3), channel_id=1, source_target_pairs={{0,1},{1,0},{2,3},{3,2},{4,5},{5,4},{6,7},{7,6},{8,9},{9,8},{10,11... | collective-permute-start | bytes 4718600 | tf_op jit(solution)/shard_map/ppermute | solution.py:226
  32.2 58.1 %collective-permute-start.7 = (bf16[3,128,2048]{2,1,0:T(8,128)(2,1)}, bf16[3,128,2048]{2,1,0:T(8,128)(2,1)}, u32[]{:S(2)}, u32[]{:S(2)}) collective-permute-start(bf16[3,128,2048]{2,1,0:T(8,128)(2,1)} %down_own.1), channel_id=1, source_target_pairs={{0,1},{1,0},{2,3},{3,2},{4,5},{5,4},{6,7},{7,6},{8,9},{9,8},{10,11... | collective-permute-start | bytes 4718600 | tf_op jit(solution)/shard_map/ppermute | solution.py:226
  33.2 57.7 %copy-start.14 = (s32[128]{0:T(128)}, s32[128]{0:T(128)S(1)}, u32[]{:S(2)}) copy-start(s32[128]{0:T(128)S(1)} %multiply_add_fusion) | copy-start | bytes 1540
  47.4 15.6 %all-to-all-start.1 = ((bf16[8,16,128]{2,1,0:T(8,128)(2,1)}), bf16[8,16,128]{2,1,0:T(8,128)(2,1)S(1)}, u32[]{:S(2)}, u32[]{:S(2)}) async-start(bf16[8,16,128]{2,1,0:T(8,128)(2,1)} %broadcast_in_dim.19), calls=%async_computation.2 | async-start | bytes 65536 | tf_op jit(solution)/shard_map/all_to_all | solution.py:262
  55.6 112.1 %all-gather.2.cloned.1.call-start = ((), (), s32[]{:S(2)}) async-start(), calls=%async_computation.8 | async-start | bytes 4128768 | tf_op jit(solution)/shard_map/all_gather | solution.py:294
  63.7 26.8 %copy-start.12 = (f32[2048]{0:T(1024)S(1)}, f32[2048]{0:T(1024)}, u32[]{:S(2)}) copy-start(f32[2048]{0:T(1024)} %param.20) | copy-start | bytes 24580
  89.1 1.4 copy-start.9
  90.3 1.4 copy-start.13
  90.9 0.8 copy-start.5
  92.4 19.4 %copy-start.11 = (f32[384,3]{0,1:T(4,128)S(1)}, f32[384,3]{0,1:T(4,128)}, u32[]{:S(2)}) copy-start(f32[384,3]{0,1:T(4,128)} %concatenate.34) | copy-start | bytes 13828
  111.6 133.4 %reduce-scatter.5.cloned.1.call-start = ((), (), s32[]{:S(2)}) async-start(), calls=%async_computation.9 | async-start | bytes 4128768 | tf_op jit(solution)/shard_map/reduce_scatter | solution.py:300
  112.7 5.8 %collective-permute-start.8 = (bf16[48,2048]{1,0:T(8,128)(2,1)S(1)}, bf16[48,2048]{1,0:T(8,128)(2,1)S(1)}, u32[]{:S(2)}, u32[]{:S(2)}) collective-permute-start(bf16[48,2048]{1,0:T(8,128)(2,1)S(1)} %reshape.177), channel_id=1, source_target_pairs={{0,2},{2,4},{4,6},{6,8},{8,10},{10,12},{12,14},{14,0},{1,3},{3,5},... | collective-permute-start | bytes 589832 | tf_op jit(solution)/shard_map/ppermute | solution.py:94
  112.7 5.7 %collective-permute-start.9 = (bf16[48,2048]{1,0:T(8,128)(2,1)S(1)}, bf16[48,2048]{1,0:T(8,128)(2,1)S(1)}, u32[]{:S(2)}, u32[]{:S(2)}) collective-permute-start(bf16[48,2048]{1,0:T(8,128)(2,1)S(1)} %reshape.177), channel_id=1, source_target_pairs={{0,14},{2,0},{4,2},{6,4},{8,6},{10,8},{12,10},{14,12},{1,15},{3,1}... | collective-permute-start | bytes 589832 | tf_op jit(solution)/shard_map/ppermute | solution.py:94
  115.4 35.3 %copy-start.1 = (bf16[3,2048,128]{2,1,0:T(8,128)(2,1)S(1)}, bf16[3,2048,128]{2,1,0:T(8,128)(2,1)}, u32[]{:S(2)}) copy-start(bf16[3,2048,128]{2,1,0:T(8,128)(2,1)} %gate_own.1) | copy-start | bytes 4718596
  118.5 8.5 %collective-permute-start.10 = (bf16[48,2048]{1,0:T(8,128)(2,1)S(1)}, bf16[48,2048]{1,0:T(8,128)(2,1)S(1)}, u32[]{:S(2)}, u32[]{:S(2)}) collective-permute-start(bf16[48,2048]{1,0:T(8,128)(2,1)S(1)} %collective-permute-done.8), channel_id=1, source_target_pairs={{0,2},{2,4},{4,6},{6,8},{8,10},{10,12},{12,14},{14,0},{1,3},{3,5},... | collective-permute-start | bytes 589832 | tf_op jit(solution)/shard_map/ppermute | solution.py:94
  118.5 10.1 %collective-permute-start.11 = (bf16[48,2048]{1,0:T(8,128)(2,1)S(1)}, bf16[48,2048]{1,0:T(8,128)(2,1)S(1)}, u32[]{:S(2)}, u32[]{:S(2)}) collective-permute-start(bf16[48,2048]{1,0:T(8,128)(2,1)S(1)} %collective-permute-done.9), channel_id=1, source_target_pairs={{0,14},{2,0},{4,2},{6,4},{8,6},{10,8},{12,10},{14,12},{1,15},{3,1}... | collective-permute-start | bytes 589832 | tf_op jit(solution)/shard_map/ppermute | solution.py:94
  126.9 16.4 %collective-permute-start.12 = (bf16[48,2048]{1,0:T(8,128)(2,1)S(1)}, bf16[48,2048]{1,0:T(8,128)(2,1)S(1)}, u32[]{:S(2)}, u32[]{:S(2)}) collective-permute-start(bf16[48,2048]{1,0:T(8,128)(2,1)S(1)} %collective-permute-done.10), channel_id=1, source_target_pairs={{0,2},{2,4},{4,6},{6,8},{8,10},{10,12},{12,14},{14,0},{1,3},{3,5},... | collective-permute-start | bytes 589832 | tf_op jit(solution)/shard_map/ppermute | solution.py:94
  128.5 11.2 %collective-permute-start.13 = (bf16[48,2048]{1,0:T(8,128)(2,1)S(1)}, bf16[48,2048]{1,0:T(8,128)(2,1)S(1)}, u32[]{:S(2)}, u32[]{:S(2)}) collective-permute-start(bf16[48,2048]{1,0:T(8,128)(2,1)S(1)} %collective-permute-done.11), channel_id=1, source_target_pairs={{0,14},{2,0},{4,2},{6,4},{8,6},{10,8},{12,10},{14,12},{1,15},{3,1}... | collective-permute-start | bytes 589832 | tf_op jit(solution)/shard_map/ppermute | solution.py:94
  139.7 8.3 %collective-permute-start.15 = (bf16[48,1024]{1,0:T(8,128)(2,1)S(1)}, bf16[48,1024]{1,0:T(8,128)(2,1)S(1)}, u32[]{:S(2)}, u32[]{:S(2)}) collective-permute-start(bf16[48,1024]{1,0:T(8,128)(2,1)S(1)} %slice.117), channel_id=1, source_target_pairs={{0,14},{2,0},{4,2},{6,4},{8,6},{10,8},{12,10},{14,12},{1,15},{3,1}... | collective-permute-start | bytes 294920 | tf_op jit(solution)/shard_map/ppermute | solution.py:94
  143.4 7.4 %collective-permute-start.14 = (bf16[48,1024]{1,0:T(8,128)(2,1)S(1)}, bf16[48,1024]{1,0:T(8,128)(2,1)S(1)}, u32[]{:S(2)}, u32[]{:S(2)}) collective-permute-start(bf16[48,1024]{1,0:T(8,128)(2,1)S(1)} %slice.116), channel_id=1, source_target_pairs={{0,2},{2,4},{4,6},{6,8},{8,10},{10,12},{12,14},{14,0},{1,3},{3,5},... | collective-permute-start | bytes 294920 | tf_op jit(solution)/shard_map/ppermute | solution.py:94
  167.7 1.4 copy-start.2
  169.1 1.4 copy-start.4
  186.0 4.8 %collective-permute-start.16 = (bf16[48,1024]{1,0:T(8,128)(2,1)S(1)}, bf16[48,1024]{1,0:T(8,128)(2,1)S(1)}, u32[]{:S(2)}, u32[]{:S(2)}) collective-permute-start(bf16[48,1024]{1,0:T(8,128)(2,1)S(1)} %slice.102), channel_id=1, source_target_pairs={{0,2},{2,4},{4,6},{6,8},{8,10},{10,12},{12,14},{14,0},{1,3},{3,5},... | collective-permute-start | bytes 294920 | tf_op jit(solution)/shard_map/ppermute | solution.py:94
  190.8 3.5 %collective-permute-start.20 = (bf16[48,1024]{1,0:T(8,128)(2,1)S(1)}, bf16[48,1024]{1,0:T(8,128)(2,1)S(1)}, u32[]{:S(2)}, u32[]{:S(2)}) collective-permute-start(bf16[48,1024]{1,0:T(8,128)(2,1)S(1)} %get-tuple-element.42), channel_id=1, source_target_pairs={{0,14},{2,0},{4,2},{6,4},{8,6},{10,8},{12,10},{14,12},{1,15},{3,1}... | collective-permute-start | bytes 294920 | tf_op jit(solution)/shard_map/ppermute | solution.py:94
  191.2 5.8 %collective-permute-start.17 = (bf16[48,2048]{1,0:T(8,128)(2,1)S(1)}, bf16[48,2048]{1,0:T(8,128)(2,1)S(1)}, u32[]{:S(2)}, u32[]{:S(2)}) collective-permute-start(bf16[48,2048]{1,0:T(8,128)(2,1)S(1)} %pad_maximum_fusion.3), channel_id=1, source_target_pairs={{0,2},{2,4},{4,6},{6,8},{8,10},{10,12},{12,14},{14,0},{1,3},{3,5},... | collective-permute-start | bytes 589832 | tf_op jit(solution)/shard_map/ppermute | solution.py:94
  194.3 9.8 %collective-permute-start.21 = (bf16[48,2048]{1,0:T(8,128)(2,1)S(1)}, bf16[48,2048]{1,0:T(8,128)(2,1)S(1)}, u32[]{:S(2)}, u32[]{:S(2)}) collective-permute-start(bf16[48,2048]{1,0:T(8,128)(2,1)S(1)} %pad_maximum_fusion.4), channel_id=1, source_target_pairs={{0,14},{2,0},{4,2},{6,4},{8,6},{10,8},{12,10},{14,12},{1,15},{3,1}... | collective-permute-start | bytes 589832 | tf_op jit(solution)/shard_map/ppermute | solution.py:94
  197.0 11.2 %collective-permute-start.18 = (bf16[48,2048]{1,0:T(8,128)(2,1)S(1)}, bf16[48,2048]{1,0:T(8,128)(2,1)S(1)}, u32[]{:S(2)}, u32[]{:S(2)}) collective-permute-start(bf16[48,2048]{1,0:T(8,128)(2,1)S(1)} %slice_add_fusion.2), channel_id=1, source_target_pairs={{0,2},{2,4},{4,6},{6,8},{8,10},{10,12},{12,14},{14,0},{1,3},{3,5},... | collective-permute-start | bytes 589832 | tf_op jit(solution)/shard_map/ppermute | solution.py:94
  208.3 9.3 %collective-permute-start.22 = (bf16[48,2048]{1,0:T(8,128)(2,1)S(1)}, bf16[48,2048]{1,0:T(8,128)(2,1)S(1)}, u32[]{:S(2)}, u32[]{:S(2)}) collective-permute-start(bf16[48,2048]{1,0:T(8,128)(2,1)S(1)} %get-tuple-element.40), channel_id=1, source_target_pairs={{0,14},{2,0},{4,2},{6,4},{8,6},{10,8},{12,10},{14,12},{1,15},{3,1}... | collective-permute-start | bytes 589832 | tf_op jit(solution)/shard_map/ppermute | solution.py:94
  208.4 11.5 %collective-permute-start.19 = (bf16[48,2048]{1,0:T(8,128)(2,1)S(1)}, bf16[48,2048]{1,0:T(8,128)(2,1)S(1)}, u32[]{:S(2)}, u32[]{:S(2)}) collective-permute-start(bf16[48,2048]{1,0:T(8,128)(2,1)S(1)} %get-tuple-element.39), channel_id=1, source_target_pairs={{0,2},{2,4},{4,6},{6,8},{8,10},{10,12},{12,14},{14,0},{1,3},{3,5},... | collective-permute-start | bytes 589832 | tf_op jit(solution)/shard_map/ppermute | solution.py:94
  217.6 11.1 %collective-permute-start.23 = (bf16[48,2048]{1,0:T(8,128)(2,1)S(1)}, bf16[48,2048]{1,0:T(8,128)(2,1)S(1)}, u32[]{:S(2)}, u32[]{:S(2)}) collective-permute-start(bf16[48,2048]{1,0:T(8,128)(2,1)S(1)} %slice_add_fusion.1), channel_id=1, source_target_pairs={{0,14},{2,0},{4,2},{6,4},{8,6},{10,8},{12,10},{14,12},{1,15},{3,1}... | collective-permute-start | bytes 589832 | tf_op jit(solution)/shard_map/ppermute | solution.py:94
  229.5 16.7 %all-to-all-start.4 = ((bf16[16,48,128]{2,1,0:T(8,128)(2,1)}), bf16[16,48,128]{2,1,0:T(8,128)(2,1)S(1)}, u32[]{:S(2)}, u32[]{:S(2)}) async-start(bf16[16,48,128]{2,1,0:T(8,128)(2,1)} %reshape.179), calls=%async_computation.6 | async-start | bytes 393216 | tf_op jit(solution)/shard_map/all_to_all | solution.py:287
  246.2 13.9 %copy-start.6 = (bf16[128,2048]{1,0:T(8,128)(2,1)S(1)}, bf16[128,2048]{1,0:T(8,128)(2,1)}, u32[]{:S(2)}) copy-start(bf16[128,2048]{1,0:T(8,128)(2,1)} %copy-done.5) | copy-start | bytes 1572868
  246.2 13.9 %copy-start.15 = (s32[128]{0:T(128)S(1)}, s32[128]{0:T(128)}, u32[]{:S(2)}) copy-start(s32[128]{0:T(128)} %copy-done.14) | copy-start | bytes 1540
Sparse Core Ops, SparseCore 0:
  30.5 58.5 reduce-scatter.2
  111.7 55.9 all-gather.1
  186.1 58.8 reduce-scatter.4
